TPU v7x, 512 devices: a whole 4x4x16 slice. The times are simulated.
512 devices in a mesh: sp: 128 (over z, x, core), tp: 4 (over y).
Axes of the slice: x: 4, y: 4, z: 16, core: 2. Of those that a mesh axis runs over, the one named last changes fastest.
Arguments:
- query_main: bfloat16 [16384, 2048], P('sp', 'tp'), may hold values from -6 to 6
- query_rotary: bfloat16 [16384, 1024], P('sp', 'tp'), may hold values from -7 to 7
- latent: bfloat16 [16384, 512], P('sp'), may hold values from -24 to 24
- key_rotary: bfloat16 [16384, 64], P('sp'), may hold values from -8 to 8
- key_weight: bfloat16 [512, 2048], P(None, 'tp'), may hold values from -0.25 to 0.25
- value_weight: bfloat16 [512, 2048], P(None, 'tp'), may hold values from -0.25 to 0.25
- head_output: bfloat16 [16384, 2048], P('sp', 'tp'), may hold values from -2 to 2
- output_grad: bfloat16 [16384, 2048], P('sp', 'tp'), may hold values from -128 to 128
- row_logsum: float32 [16, 16384], P('tp', 'sp'), may hold values from 3 to 16, as said below
Outputs:
- grad_query_main: float32 [16384, 2048], P('sp', 'tp')
- grad_query_rotary: float32 [16384, 1024], P('sp', 'tp')
- grad_latent: float32 [16384, 512], P('sp')
- grad_key_rotary: float32 [16384, 64], P('sp')
- grad_key_weight: float32 [512, 2048], P('sp', 'tp')
Inputs may be any that keep to these rules, and one draw needn't show every extreme that they name: With p the place of token i in its sequence and q = i % 128, row_logsum[h, i] minus the logarithm of (p + 1 + 54 (q + 1)) lies between -0.3 and 1.5.
All inputs are finite; a program needn't handle non-finite values.
Results may differ from a plain program's by a relative error of at most 0.003.
The roundings to bfloat16 on the way count: a program that leaves them out, or rounds other values in their place, can miss the bound.
Values may be sent and summed in bfloat16 or wider, within the bound.
A program may use at most 64 MiB of HBM per device.

v0:
```python
import jax
import jax.numpy as jnp
from jax import lax
from jax.sharding import Mesh
from jax.sharding import PartitionSpec as P

SEQ_DEVICES = 32
SP = ("sp_0", "sp_1", "sp_2")


def shifted(shard, axis, by):
    peers = lax.axis_size(axis)
    pairs = [(i, i + by) for i in range(peers) if 0 <= i + by < peers]
    return lax.ppermute(shard, axis, pairs)


def from_behind(block, axis, distance):
    devices = range(lax.axis_size(axis))
    route = [((i - distance) % len(devices), i) for i in devices]
    return lax.ppermute(block, axis, route)


def from_everyone(shard, axis):
    peers = lax.axis_size(axis)
    return lax.all_to_all(
        jnp.broadcast_to(shard[None], (peers, *shard.shape)), axis, 0, 0, tiled=True
    )


def of_everyone(shard, axis):
    return from_everyone(shard, axis).sum(axis=0)


def in_one(arrays, axis):
    ends = [0]
    for a in arrays:
        ends.append(ends[-1] + a.size)
    so_far = of_everyone(jnp.concatenate([a.ravel() for a in arrays]), axis)
    return tuple((so_far[b:e].reshape(a.shape) for a, b, e in zip(arrays, ends, ends[1:])))


def sum_in_order(tiles, axes, turns):
    inside = tiles.shape[1:]
    tiles = tiles.reshape(*(lax.axis_size(a) for a in axes), *inside)
    tiles = jnp.moveaxis(tiles, turns, range(len(axes))).reshape(-1, *inside)
    for k in turns:
        tiles = lax.psum_scatter(tiles, axes[k], scatter_dimension=0, tiled=True)
    return tiles[0]


def split_up(shard, dim, peers):
    shape = shard.shape
    tiles = shard.reshape(*shape[:dim], peers, shape[dim] // peers, *shape[dim + 1 :])
    return jnp.moveaxis(tiles, dim, 0)


def summed_rows(shard, axes, turns, dim):
    peers = lax.axis_size(axes)
    return sum_in_order(split_up(shard, dim, peers), axes, turns)


def per_device(
    query_main,
    query_rotary,
    latent,
    key_rotary,
    key_weight,
    value_weight,
    head_output,
    output_grad,
    row_logsum,
):
    devices = lax.axis_size(SP)
    my_index = lax.axis_index(SP)
    group_span = min(SEQ_DEVICES, devices)
    lead_span = group_span // 4
    own_sequence = (my_index + lead_span) // group_span
    heads_here, tok_rows = row_logsum.shape
    lat_width = latent.shape[1]
    rot_width = key_rotary.shape[1]
    main_width = key_weight.shape[1] // heads_here
    value_width = value_weight.shape[1] // heads_here
    factor = (main_width + rot_width) ** (-0.5)
    main_query = query_main.reshape(tok_rows, heads_here, main_width)
    rot_query = query_rotary.reshape(tok_rows, heads_here, rot_width)
    key_proj = key_weight.reshape(lat_width, heads_here, main_width)
    value_proj = value_weight.reshape(lat_width, heads_here, value_width)
    grad_heads = output_grad.reshape(tok_rows, heads_here, value_width)
    query_latent = jnp.einsum(
        "thd,lhd->thl", main_query, key_proj, preferred_element_type=jnp.float32
    ).astype(jnp.bfloat16)
    grad_rows = jnp.einsum(
        "thd,lhd->thl", grad_heads, value_proj, preferred_element_type=jnp.float32
    ).astype(jnp.bfloat16)
    row_terms = jnp.sum(
        head_output.reshape(tok_rows, heads_here, value_width).astype(jnp.float32)
        * grad_heads.astype(jnp.float32),
        axis=2,
    )
    row_logs = row_logsum.T
    query_place = my_index * tok_rows + jnp.arange(tok_rows)

    def attend_block(state, key_block, grad_block, block_index, first_row):
        mixed_sum, rot_sum = state
        lat_block, rot_block = key_block
        acc_lat, acc_rot = grad_block
        key_place = block_index * tok_rows + first_row + jnp.arange(lat_block.shape[0])
        seen = key_place[None, :] <= query_place[:, None]
        scores = jnp.einsum(
            "thl,kl->thk", query_latent, lat_block, preferred_element_type=jnp.float32
        )
        scores = scores + jnp.einsum(
            "thr,kr->thk", rot_query, rot_block, preferred_element_type=jnp.float32
        )
        weights = jnp.where(seen[:, None, :], jnp.exp(factor * scores - row_logs[:, :, None]), 0.0)
        slopes = jnp.einsum("thl,kl->thk", grad_rows, lat_block, preferred_element_type=jnp.float32)
        dscores = weights * (slopes - row_terms[:, :, None])
        weights_low = weights.astype(jnp.bfloat16)
        dscores_low = dscores.astype(jnp.bfloat16)
        mixed_sum = mixed_sum + jnp.einsum(
            "thk,kl->thl", dscores_low, lat_block, preferred_element_type=jnp.float32
        )
        rot_sum = rot_sum + jnp.einsum(
            "thk,kr->thr", dscores_low, rot_block, preferred_element_type=jnp.float32
        )
        part_lat = factor * jnp.einsum(
            "thk,thl->kl", dscores_low, query_latent, preferred_element_type=jnp.float32
        )
        part_lat = part_lat + jnp.einsum(
            "thk,thl->kl", weights_low, grad_rows, preferred_element_type=jnp.float32
        )
        part_rot = factor * jnp.einsum(
            "thk,thr->kr", dscores_low, rot_query, preferred_element_type=jnp.float32
        )
        return ((mixed_sum, rot_sum), (acc_lat + part_lat, acc_rot + part_rot))

    def visit_block(state, key_block, grad_block, block_index, first_row):
        useful = ((block_index + lead_span) // group_span == own_sequence) & (
            block_index <= my_index
        )

        def work(operand):
            return attend_block(operand[0], key_block, operand[1], block_index, first_row)

        def skip(operand):
            return operand

        return lax.cond(useful, work, skip, (state, grad_block))

    zero_state = (
        jnp.zeros((tok_rows, heads_here, lat_width), jnp.float32),
        jnp.zeros((tok_rows, heads_here, rot_width), jnp.float32),
    )
    zero_grads = (
        jnp.zeros((tok_rows, lat_width), jnp.float32),
        jnp.zeros((tok_rows, rot_width), jnp.float32),
    )

    def forward_step(step, carry):
        state, key_block, grad_block = carry
        state, grad_block = visit_block(
            state, key_block, grad_block, (my_index - step) % devices, 0
        )
        key_block = shifted((key_block[0], key_block[1]), SP, 1)
        grad_block = from_behind((grad_block[0], grad_block[1]), SP, 1)
        return (state, key_block, grad_block)

    state, key_block, grad_block = lax.fori_loop(
        0, group_span - 1, forward_step, (zero_state, (latent, key_rotary), zero_grads)
    )
    state, grad_block = visit_block(
        state, key_block, grad_block, (my_index + 1 - group_span) % devices, 0
    )
    lat_grad, rot_grad = from_behind((grad_block[0], grad_block[1]), SP, 1 - group_span)
    lat_grad, rot_grad = in_one((lat_grad, rot_grad), "tp")
    mixed_sum, rot_sum = state
    mixed_low = mixed_sum.astype(jnp.bfloat16)
    grad_main = factor * jnp.einsum(
        "thl,lhd->thd", mixed_low, key_proj, preferred_element_type=jnp.float32
    )
    term = jnp.einsum("thl,thd->lhd", mixed_low, main_query, preferred_element_type=jnp.float32)
    grad_weight = summed_rows(
        factor * term.reshape(lat_width // devices * lax.axis_size(SP), heads_here * main_width),
        SP,
        (2, 0, 1),
        0,
    )
    return (
        grad_main.reshape(tok_rows, heads_here * main_width),
        (factor * rot_sum).reshape(tok_rows, heads_here * rot_width),
        lat_grad,
        rot_grad,
        grad_weight,
    )


def solution(mesh):
    finer = Mesh(mesh.devices.reshape(16, 4, 2, mesh.shape["tp"]), ("sp_0", "sp_1", "sp_2", "tp"))
    return jax.shard_map(
        per_device,
        mesh=finer,
        in_specs=(
            P(SP, "tp"),
            P(SP, "tp"),
            P(SP, None),
            P(SP, None),
            P(None, "tp"),
            P(None, "tp"),
            P(SP, "tp"),
            P(SP, "tp"),
            P("tp", SP),
        ),
        out_specs=(P(SP, "tp"), P(SP, "tp"), P(SP, None), P(SP, None), P(SP, "tp")),
        check_vma=False,
    )
```

profile of v0, /device:TPU:8, one launch (start us, length us, event | category | flops | bytes accessed | tf_op | source)
XLA Modules:
  0.0 737.1 jit_solution(15190983055127998566)
XLA Ops:
  12.4 477.9 %while.26 = (s32[]{:T(128)}, f32[128,4,512]{2,0,1:T(8,128)S(1)}, f32[128,4,64]{0,2,1:T(8,128)}, bf16[128,512]{1,0:T(8,128)(2,1)S(1)}, bf16[128,64]{0,1:T(8,128)(...) while((s32[]{:T(128)}, f32[128,4,512]{2,0,1:T(8,128)S(1)}, ...), condition=%wide.region_4.5_spmd.clone, body=%wide.region_1.4_spmd.clone.sunk | while | flops 361759008 | bytes 10788718 | solution.py:168
  27.1 7.1 collective-permute-done.3
  68.4 5.6 collective-permute-start.3
  87.1 7.6 %collective-permute-start.1 = (bf16[128,64]{0,1:T(8,128)(2,1)S(1)}, bf16[128,64]{0,1:T(8,128)(2,1)S(1)}, u32[]{:S(2)}, u32[]{:S(2)}) collective-permute-start(bf16[128,64]{0,1:T(8,128)(2,1)S(1)} %copy.198), channel_id=1, source_target_pairs={{0,4},{4,8},{8,12},{12,16},{16,20},{20,24},{24,28},{28,32},{32,36}... | collective-permute-start | bytes 49160 | tf_op jit(solution)/shard_map/while/body/eval_jaxpr/ppermute | solution.py:14
  152.0 6.0 collective-permute-start.1
  167.3 7.4 %collective-permute-start.1 = (bf16[128,64]{0,1:T(8,128)(2,1)S(1)}, bf16[128,64]{0,1:T(8,128)(2,1)S(1)}, u32[]{:S(2)}, u32[]{:S(2)}) collective-permute-start(bf16[128,64]{0,1:T(8,128)(2,1)S(1)} %copy.198), channel_id=1, source_target_pairs={{0,4},{4,8},{8,12},{12,16},{16,20},{20,24},{24,28},{28,32},{32,36}... | collective-permute-start | bytes 49160 | tf_op jit(solution)/shard_map/while/body/eval_jaxpr/ppermute | solution.py:14
  199.0 6.0 collective-permute-start.1
  215.7 6.0 collective-permute-start.1
  232.3 6.3 collective-permute-start.1
  247.9 6.0 collective-permute-start.1
  263.5 6.0 collective-permute-start.1
  280.2 6.0 collective-permute-start.1
  296.8 6.3 collective-permute-start.1
  312.4 5.3 collective-permute-start.1
  327.0 7.1 collective-permute-start.1
  343.8 6.0 collective-permute-start.1
  452.6 6.0 collective-permute-start.1
  468.0 5.5 collective-permute-start.1
  490.3 29.5 %collective-permute-start.4 = (f32[128,512]{1,0:T(8,128)S(1)}, f32[128,512]{1,0:T(8,128)S(1)}, u32[]{:S(2)}, u32[]{:S(2)}) collective-permute-start(f32[128,512]{1,0:T(8,128)S(1)} %get-tuple-element.740), channel_id=1, source_target_pairs={{124,0},{128,4},{132,8},{136,12},{140,16},{144,20},{148,24},{152,2... | collective-permute-start | bytes 786440 | tf_op jit(solution)/shard_map/ppermute | solution.py:20
  519.9 7.0 collective-permute-start.5
  532.8 9.7 %collective-permute-done.5 = f32[128,64]{0,1:T(8,128)S(1)} collective-permute-done((f32[128,64]{0,1:T(8,128)S(1)}, f32[128,64]{0,1:T(8,128)S(1)}, u32[]{:S(2)}, u32[]{:S(2)}) %collective-permute-start.5) | collective-permute-done | bytes 32800 | tf_op jit(solution)/shard_map/ppermute | solution.py:20
  551.3 18.9 %all-reduce.6.cloned.1.call-done = f32[128,4,512]{2,1,0:T(4,128)} async-done(((f32[128,4,512]{2,1,0:T(4,128)}), f32[128,4,512]{2,1,0:T(4,128)}) %all-reduce.6.cloned.1.call-update) | async-done | bytes 1048592
  580.8 130.5 %all-reduce.8.cloned.1.call-done = f32[64,4,512]{2,1,0:T(4,128)} async-done(((f32[64,4,512]{2,1,0:T(4,128)}), f32[64,4,512]{2,1,0:T(4,128)}) %all-reduce.8.cloned.1.call-update) | async-done | bytes 524304
  712.1 17.0 %all-reduce.2 = f32[4,4,512]{2,1,0:T(4,128)S(1)} all-reduce(f32[4,4,512]{2,1,0:T(4,128)S(1)} %constant_dynamic-slice_fusion), channel_id=4, replica_groups=mesh['sp_0'=16,'sp_1'=4,'sp_2'=2,'tp'=4] {'sp_1'}, use_global_device_ids=true, to_apply=%region_10.11.clone | all-reduce | flops 8192 | bytes 65536
  (501 shorter events, 401.2 us)
Async XLA Ops:
  7.2 563.0 %all-reduce.6.cloned.1.call-start = ((), (), s32[]{:S(2)}) async-start(), calls=%async_computation.1 | async-start | bytes 2097152
  16.2 18.7 %collective-permute-start.2 = (f32[128,512]{1,0:T(8,128)S(1)}, f32[128,512]{1,0:T(8,128)S(1)}, u32[]{:S(2)}, u32[]{:S(2)}) collective-permute-start(f32[128,512]{1,0:T(8,128)S(1)} %get-tuple-element.872), channel_id=1, source_target_pairs={{508,0},{0,4},{4,8},{8,12},{12,16},{16,20},{20,24},{24,28},{28,32}... | collective-permute-start | bytes 786440 | tf_op jit(solution)/shard_map/while/body/eval_jaxpr/ppermute | solution.py:20
  18.1 16.9 %collective-permute-start = (bf16[128,512]{1,0:T(8,128)(2,1)S(1)}, bf16[128,512]{1,0:T(8,128)(2,1)S(1)}, u32[]{:S(2)}, u32[]{:S(2)}) collective-permute-start(bf16[128,512]{1,0:T(8,128)(2,1)S(1)} %copy.197), channel_id=1, source_target_pairs={{0,4},{4,8},{8,12},{12,16},{16,20},{20,24},{24,28},{28,32},{32,36}... | collective-permute-start | bytes 393224 | tf_op jit(solution)/shard_map/while/body/eval_jaxpr/ppermute | solution.py:14
  48.0 15.3 %collective-permute-start.2 = (f32[128,512]{1,0:T(8,128)S(1)}, f32[128,512]{1,0:T(8,128)S(1)}, u32[]{:S(2)}, u32[]{:S(2)}) collective-permute-start(f32[128,512]{1,0:T(8,128)S(1)} %get-tuple-element.872), channel_id=1, source_target_pairs={{508,0},{0,4},{4,8},{8,12},{12,16},{16,20},{20,24},{24,28},{28,32}... | collective-permute-start | bytes 786440 | tf_op jit(solution)/shard_map/while/body/eval_jaxpr/ppermute | solution.py:20
  63.4 15.3 %collective-permute-start.2 = (f32[128,512]{1,0:T(8,128)S(1)}, f32[128,512]{1,0:T(8,128)S(1)}, u32[]{:S(2)}, u32[]{:S(2)}) collective-permute-start(f32[128,512]{1,0:T(8,128)S(1)} %get-tuple-element.872), channel_id=1, source_target_pairs={{508,0},{0,4},{4,8},{8,12},{12,16},{16,20},{20,24},{24,28},{28,32}... | collective-permute-start | bytes 786440 | tf_op jit(solution)/shard_map/while/body/eval_jaxpr/ppermute | solution.py:20
  78.9 16.6 %collective-permute-start.2 = (f32[128,512]{1,0:T(8,128)S(1)}, f32[128,512]{1,0:T(8,128)S(1)}, u32[]{:S(2)}, u32[]{:S(2)}) collective-permute-start(f32[128,512]{1,0:T(8,128)S(1)} %get-tuple-element.872), channel_id=1, source_target_pairs={{508,0},{0,4},{4,8},{8,12},{12,16},{16,20},{20,24},{24,28},{28,32}... | collective-permute-start | bytes 786440 | tf_op jit(solution)/shard_map/while/body/eval_jaxpr/ppermute | solution.py:20
  95.6 15.7 %collective-permute-start.2 = (f32[128,512]{1,0:T(8,128)S(1)}, f32[128,512]{1,0:T(8,128)S(1)}, u32[]{:S(2)}, u32[]{:S(2)}) collective-permute-start(f32[128,512]{1,0:T(8,128)S(1)} %get-tuple-element.872), channel_id=1, source_target_pairs={{508,0},{0,4},{4,8},{8,12},{12,16},{16,20},{20,24},{24,28},{28,32}... | collective-permute-start | bytes 786440 | tf_op jit(solution)/shard_map/while/body/eval_jaxpr/ppermute | solution.py:20
  111.5 16.8 %collective-permute-start.2 = (f32[128,512]{1,0:T(8,128)S(1)}, f32[128,512]{1,0:T(8,128)S(1)}, u32[]{:S(2)}, u32[]{:S(2)}) collective-permute-start(f32[128,512]{1,0:T(8,128)S(1)} %get-tuple-element.872), channel_id=1, source_target_pairs={{508,0},{0,4},{4,8},{8,12},{12,16},{16,20},{20,24},{24,28},{28,32}... | collective-permute-start | bytes 786440 | tf_op jit(solution)/shard_map/while/body/eval_jaxpr/ppermute | solution.py:20
  128.5 16.3 %collective-permute-start.2 = (f32[128,512]{1,0:T(8,128)S(1)}, f32[128,512]{1,0:T(8,128)S(1)}, u32[]{:S(2)}, u32[]{:S(2)}) collective-permute-start(f32[128,512]{1,0:T(8,128)S(1)} %get-tuple-element.872), channel_id=1, source_target_pairs={{508,0},{0,4},{4,8},{8,12},{12,16},{16,20},{20,24},{24,28},{28,32}... | collective-permute-start | bytes 786440 | tf_op jit(solution)/shard_map/while/body/eval_jaxpr/ppermute | solution.py:20
  159.0 16.6 %collective-permute-start.2 = (f32[128,512]{1,0:T(8,128)S(1)}, f32[128,512]{1,0:T(8,128)S(1)}, u32[]{:S(2)}, u32[]{:S(2)}) collective-permute-start(f32[128,512]{1,0:T(8,128)S(1)} %get-tuple-element.872), channel_id=1, source_target_pairs={{508,0},{0,4},{4,8},{8,12},{12,16},{16,20},{20,24},{24,28},{28,32}... | collective-permute-start | bytes 786440 | tf_op jit(solution)/shard_map/while/body/eval_jaxpr/ppermute | solution.py:20
  175.7 15.8 %collective-permute-start.2 = (f32[128,512]{1,0:T(8,128)S(1)}, f32[128,512]{1,0:T(8,128)S(1)}, u32[]{:S(2)}, u32[]{:S(2)}) collective-permute-start(f32[128,512]{1,0:T(8,128)S(1)} %get-tuple-element.872), channel_id=1, source_target_pairs={{508,0},{0,4},{4,8},{8,12},{12,16},{16,20},{20,24},{24,28},{28,32}... | collective-permute-start | bytes 786440 | tf_op jit(solution)/shard_map/while/body/eval_jaxpr/ppermute | solution.py:20
  206.4 16.6 %collective-permute-start.2 = (f32[128,512]{1,0:T(8,128)S(1)}, f32[128,512]{1,0:T(8,128)S(1)}, u32[]{:S(2)}, u32[]{:S(2)}) collective-permute-start(f32[128,512]{1,0:T(8,128)S(1)} %get-tuple-element.872), channel_id=1, source_target_pairs={{508,0},{0,4},{4,8},{8,12},{12,16},{16,20},{20,24},{24,28},{28,32}... | collective-permute-start | bytes 786440 | tf_op jit(solution)/shard_map/while/body/eval_jaxpr/ppermute | solution.py:20
  223.1 16.2 %collective-permute-start.2 = (f32[128,512]{1,0:T(8,128)S(1)}, f32[128,512]{1,0:T(8,128)S(1)}, u32[]{:S(2)}, u32[]{:S(2)}) collective-permute-start(f32[128,512]{1,0:T(8,128)S(1)} %get-tuple-element.872), channel_id=1, source_target_pairs={{508,0},{0,4},{4,8},{8,12},{12,16},{16,20},{20,24},{24,28},{28,32}... | collective-permute-start | bytes 786440 | tf_op jit(solution)/shard_map/while/body/eval_jaxpr/ppermute | solution.py:20
  239.6 15.8 %collective-permute-start.2 = (f32[128,512]{1,0:T(8,128)S(1)}, f32[128,512]{1,0:T(8,128)S(1)}, u32[]{:S(2)}, u32[]{:S(2)}) collective-permute-start(f32[128,512]{1,0:T(8,128)S(1)} %get-tuple-element.872), channel_id=1, source_target_pairs={{508,0},{0,4},{4,8},{8,12},{12,16},{16,20},{20,24},{24,28},{28,32}... | collective-permute-start | bytes 786440 | tf_op jit(solution)/shard_map/while/body/eval_jaxpr/ppermute | solution.py:20
  270.9 16.6 %collective-permute-start.2 = (f32[128,512]{1,0:T(8,128)S(1)}, f32[128,512]{1,0:T(8,128)S(1)}, u32[]{:S(2)}, u32[]{:S(2)}) collective-permute-start(f32[128,512]{1,0:T(8,128)S(1)} %get-tuple-element.872), channel_id=1, source_target_pairs={{508,0},{0,4},{4,8},{8,12},{12,16},{16,20},{20,24},{24,28},{28,32}... | collective-permute-start | bytes 786440 | tf_op jit(solution)/shard_map/while/body/eval_jaxpr/ppermute | solution.py:20
  287.6 16.4 %collective-permute-start.2 = (f32[128,512]{1,0:T(8,128)S(1)}, f32[128,512]{1,0:T(8,128)S(1)}, u32[]{:S(2)}, u32[]{:S(2)}) collective-permute-start(f32[128,512]{1,0:T(8,128)S(1)} %get-tuple-element.872), channel_id=1, source_target_pairs={{508,0},{0,4},{4,8},{8,12},{12,16},{16,20},{20,24},{24,28},{28,32}... | collective-permute-start | bytes 786440 | tf_op jit(solution)/shard_map/while/body/eval_jaxpr/ppermute | solution.py:20
  304.2 15.7 %collective-permute-start.2 = (f32[128,512]{1,0:T(8,128)S(1)}, f32[128,512]{1,0:T(8,128)S(1)}, u32[]{:S(2)}, u32[]{:S(2)}) collective-permute-start(f32[128,512]{1,0:T(8,128)S(1)} %get-tuple-element.872), channel_id=1, source_target_pairs={{508,0},{0,4},{4,8},{8,12},{12,16},{16,20},{20,24},{24,28},{28,32}... | collective-permute-start | bytes 786440 | tf_op jit(solution)/shard_map/while/body/eval_jaxpr/ppermute | solution.py:20
  335.1 15.8 %collective-permute-start.2 = (f32[128,512]{1,0:T(8,128)S(1)}, f32[128,512]{1,0:T(8,128)S(1)}, u32[]{:S(2)}, u32[]{:S(2)}) collective-permute-start(f32[128,512]{1,0:T(8,128)S(1)} %get-tuple-element.872), channel_id=1, source_target_pairs={{508,0},{0,4},{4,8},{8,12},{12,16},{16,20},{20,24},{24,28},{28,32}... | collective-permute-start | bytes 786440 | tf_op jit(solution)/shard_map/while/body/eval_jaxpr/ppermute | solution.py:20
  351.2 15.4 %collective-permute-start.2 = (f32[128,512]{1,0:T(8,128)S(1)}, f32[128,512]{1,0:T(8,128)S(1)}, u32[]{:S(2)}, u32[]{:S(2)}) collective-permute-start(f32[128,512]{1,0:T(8,128)S(1)} %get-tuple-element.872), channel_id=1, source_target_pairs={{508,0},{0,4},{4,8},{8,12},{12,16},{16,20},{20,24},{24,28},{28,32}... | collective-permute-start | bytes 786440 | tf_op jit(solution)/shard_map/while/body/eval_jaxpr/ppermute | solution.py:20
  460.0 15.4 %collective-permute-start.2 = (f32[128,512]{1,0:T(8,128)S(1)}, f32[128,512]{1,0:T(8,128)S(1)}, u32[]{:S(2)}, u32[]{:S(2)}) collective-permute-start(f32[128,512]{1,0:T(8,128)S(1)} %get-tuple-element.872), channel_id=1, source_target_pairs={{508,0},{0,4},{4,8},{8,12},{12,16},{16,20},{20,24},{24,28},{28,32}... | collective-permute-start | bytes 786440 | tf_op jit(solution)/shard_map/while/body/eval_jaxpr/ppermute | solution.py:20
  490.3 52.4 %collective-permute-start.4 = (f32[128,512]{1,0:T(8,128)S(1)}, f32[128,512]{1,0:T(8,128)S(1)}, u32[]{:S(2)}, u32[]{:S(2)}) collective-permute-start(f32[128,512]{1,0:T(8,128)S(1)} %get-tuple-element.740), channel_id=1, source_target_pairs={{124,0},{128,4},{132,8},{136,12},{140,16},{144,20},{148,24},{152,2... | collective-permute-start | bytes 786440 | tf_op jit(solution)/shard_map/ppermute | solution.py:20
  519.9 22.6 %collective-permute-start.5 = (f32[128,64]{0,1:T(8,128)S(1)}, f32[128,64]{0,1:T(8,128)S(1)}, u32[]{:S(2)}, u32[]{:S(2)}) collective-permute-start(f32[128,64]{0,1:T(8,128)S(1)} %get-tuple-element.741), channel_id=1, source_target_pairs={{124,0},{128,4},{132,8},{136,12},{140,16},{144,20},{148,24},{152,2... | collective-permute-start | bytes 98312 | tf_op jit(solution)/shard_map/ppermute | solution.py:20
  544.4 33.7 %all-to-all-start = ((f32[4,1,73728]{2,1,0:T(1,128)}), f32[4,1,73728]{2,1,0:T(1,128)S(1)}, u32[]{:S(2)}, u32[]{:S(2)}) async-start(f32[4,1,73728]{2,1,0:T(1,128)} %broadcast_in_dim.52), calls=%async_computation | async-start | bytes 2359296 | tf_op jit(solution)/shard_map/all_to_all | solution.py:25
  549.3 162.0 %all-reduce.8.cloned.1.call-start = ((), (), s32[]{:S(2)}) async-start(), calls=%async_computation.2 | async-start | bytes 1048576
  (118 other events, 1116.9 us)
Sparse Core Ops, SparseCore 0:
  532.9 37.1 all-reduce.5
  572.5 138.7 all-reduce.7
where the time goes:
time: 744 us; the launch traced here: 737 us
  starting transfers between devices  435 us (58%)
  waiting for transfers between devices  210 us (28%)
  local copies, waits for them, and re-layouts  46 us (6%)
  blocking collectives  17 us (2%)
  between operations  15.7 us (2%)
    ppermute x62, starting transfers between devices, shifted(): return lax.ppermute(shard, axis, pairs)  262 us
    ppermute x64, starting transfers between devices, from_behind(): return lax.ppermute(block, axis, route)  168 us
    unnamed x4, waiting for transfers between devices  149 us
    ppermute x64, waiting for transfers between devices, from_behind(): return lax.ppermute(block, axis, route)  59.9 us
    while x124, local copies, waits for them, and re-layouts  24.5 us
    unnamed x1, blocking collectives  17 us
  transfers between devices with their start and end apart: 129, of which 28 were waited for; matrix products, arithmetic and copies ran while one was open for 6% of the time, Pallas kernels for 0%

commit v1 on v0

v1 whole, which is shorter than its diff:
```python
import functools

import jax
import jax.numpy as jnp
from jax import lax
from jax.experimental import pallas as pl
from jax.experimental.pallas import tpu as pltpu
from jax.sharding import Mesh
from jax.sharding import PartitionSpec as P

MESH = pl.DeviceIdType.MESH
SP = ("z", "x", "c")
F32 = jnp.float32
BF16 = jnp.bfloat16
WIDE = 640
NT = (((1,), (1,)), ((), ()))
TN = (((0,), (0,)), ((), ()))


def dot(a, b, dims=(((1,), (0,)), ((), ()))):
    return lax.dot_general(a, b, dims, preferred_element_type=F32)


def body(
    qm, qr, kcat, kw, vw, ho, og, ls,
    o_main, o_rot, o_lat, o_krot, o_weight,
    keys, part, dsum, y1s, y1r, y2s, y2r, xs, xr, zs, zr, fin,
    mix, qc, gr, stats, low, term, termr, wx0, wxs, wxr, wz, wzr, wf, wfr,
    s_loc, s_kz, r_kz, s_kx, r_kx, s_kd, r_kd, s_d, r_d, s_y1, r_y1, s_y2, r_y2,
    s_x, r_x, s_z, r_z, s_f, r_f, s_t, r_t, s_wx, r_wx, s_wz, r_wz, s_wf, r_wf,
):
    z, x, c, y = (lax.axis_index(a) for a in ("z", "x", "c", "y"))
    factor = 192.0 ** (-0.5)
    zp = jnp.where(z < 3, z, (z + 1) % 4)
    planes = jnp.where(z < 3, 3, jnp.where(z < 15, 4, 1))
    more = planes - 1 - zp
    sib = {"c": 1 - c}
    x1, x3, x2 = x + 1 - 2 * (x % 2), 3 - x, (x + 2) % 4
    y1, y3, y2 = y + 1 - 2 * (y % 2), 3 - y, (y + 2) % 4

    def remote(src, dst, ss, rs, dev):
        return pltpu.make_async_remote_copy(
            src_ref=src, dst_ref=dst, send_sem=ss, recv_sem=rs, device_id=dev, device_id_type=MESH
        )

    def c_kz(s):
        return remote(keys.at[s, 0, 0], keys.at[s + 1, 0, 0], s_kz.at[s], r_kz.at[s + 1], {"z": z + 1})

    def c_kzr(s):
        return remote(keys.at[s, 0, 0], keys.at[s, 0, 0], s_kz.at[s], r_kz.at[s], {"z": z - 1})

    def c_kx(s, j):
        dev = {"x": x1} if j == 1 else {"x": x3}
        return remote(keys.at[s, 0, 0], keys.at[s, j, 0], s_kx.at[s, j - 1], r_kx.at[s, j - 1], dev)

    def c_kh(s, j):
        src, rows, dev = (1, 0, {"x": x3}) if j == 0 else (2, 64, {"x": x1})
        return remote(
            keys.at[s, src, 0, pl.ds(rows, 64)], keys.at[s, 3, 0, pl.ds(rows, 64)],
            s_kx.at[s, 2 + j], r_kx.at[s, 2 + j], dev,
        )

    def c_kd(s, j):
        return remote(keys.at[s, j, 0], keys.at[s, j, 1], s_kd.at[s, j], r_kd.at[s, j], sib)

    def c_d(s, j):
        return remote(part.at[s, j, 1], dsum.at[s, j], s_d.at[s, j], r_d.at[s, j], sib)

    def c_y1(s, g):
        dev = {"y": y1} if g == 0 else {"y": y3}
        return remote(y1s.at[s, g], y1r.at[s, g], s_y1.at[s, g], r_y1.at[s, g], dev)

    def c_y2(s, g):
        dev = {"y": y3} if g == 0 else {"y": y1}
        return remote(y2s.at[s, g], y2r.at[s, g], s_y2.at[s, g], r_y2.at[s, g], dev)

    def c_x(s, j):
        dev = {"x": (x1, x3, x2)[j - 1]}
        return remote(xs.at[s, j], xr.at[s, j], s_x.at[s, j], r_x.at[s, j], dev)

    def c_z(s):
        return remote(zs.at[s], zr.at[s], s_z.at[s], r_z.at[s], {"z": z - s})

    def c_zr(s):
        return remote(zs.at[s], zr.at[s], s_z.at[s], r_z.at[s], {"z": z + s})

    def c_f(j):
        dev = {"y": (y1, y3, y2)[j - 1]}
        return remote(fin.at[0], fin.at[j], s_f.at[j], r_f.at[j], dev)

    c_t = remote(term.at[1], termr, s_t, r_t, sib)

    def c_wx(j):
        dev = {"x": (x1, x3, x2)[j - 1]}
        return remote(wxs.at[j], wxr.at[j], s_wx.at[j], r_wx.at[j], dev)

    def c_wz(d):
        to = (z + d) % 16
        return remote(wz.at[to], wzr.at[d], s_wz.at[d], r_wz.at[d], {"z": to})

    c_wf = remote(wf, wfr, s_wf, r_wf, sib)

    load = pltpu.make_async_copy(kcat, keys.at[0, 0, 0], s_loc)
    load.start()
    barrier = pltpu.get_barrier_semaphore()
    for dev in (sib, {"x": x1}, {"x": x2}, {"x": x3}, {"y": y1}, {"y": y2}, {"y": y3}):
        pl.semaphore_signal(barrier, inc=1, device_id=dev, device_id_type=MESH)

    def greet(d, carry):
        pl.semaphore_signal(barrier, inc=1, device_id={"z": (z + d) % 16}, device_id_type=MESH)
        return carry

    lax.fori_loop(1, 16, greet, 0)
    load.wait()
    pl.semaphore_wait(barrier, 22)

    def pass_on(s):
        @pl.when(more > 0)
        def _():
            c_kz(s).start()

        c_kx(s, 1).start()
        c_kx(s, 2).start()
        c_kd(s, 0).start()

    pass_on(0)

    ones = jnp.ones((8, 128), F32)
    for h in range(4):
        cols = pl.ds(h * 128, 128)
        rows = pl.ds(h * 128, 128)
        qc[rows, 0:512] = dot(qm[:, cols], kw[:, cols], NT).astype(BF16)
        gr[rows, :] = dot(og[:, cols], vw[:, cols], NT).astype(BF16)
        rot = qr[:, h * 64 : (h + 1) * 64]
        qc[rows, 512:WIDE] = jnp.concatenate([rot, jnp.zeros((128, 64), BF16)], axis=1)
        prod = ho[:, cols].astype(F32) * og[:, cols].astype(F32)
        sums = lax.dot_general(
            ones, prod, NT, precision=lax.Precision.HIGHEST, preferred_element_type=F32
        )
        stats[1:2, cols] = sums[0:1, :]
        stats[0:1, cols] = ls[h : h + 1, :]
    mix[...] = jnp.zeros_like(mix)

    def tile(s, j):
        kt = keys[s, j].reshape(256, WIDE)
        turn = jnp.where(j == 0, x, jnp.where(j == 1, x1, jnp.where(j == 2, x3, x2)))
        far = jnp.where(s > 0, 1 << 20, 0)
        first = (2 * turn + c) * 128 - far
        second = (2 * turn + 1 - c) * 128 - 128 - far
        k_row = lax.broadcasted_iota(jnp.int32, (256, 1), 0)
        k_place = jnp.where(k_row < 128, k_row + first, k_row + second)
        q_place = lax.broadcasted_iota(jnp.int32, (1, 512), 1) % 128 + (2 * x + c) * 128
        scores = dot(kt, qc[...], NT)
        weights = jnp.where(k_place <= q_place, jnp.exp(factor * scores - stats[0:1, :]), 0.0)
        slopes = dot(kt[:, 0:512], gr[...], NT)
        dscores = weights * (slopes - stats[1:2, :])
        w_low = weights.astype(BF16)
        d_low = dscores.astype(BF16)
        mix[...] += dot(kt, d_low, TN)
        main = factor * dot(d_low, qc[:, 0:512]) + dot(w_low, gr[...])
        rest = factor * dot(d_low, qc[:, 512:WIDE])
        part[s, j, :, :, 0:512] = main.reshape(2, 128, 512)
        part[s, j, :, :, 512:WIDE] = rest.reshape(2, 128, 128)

    def own(s, j, yy):
        rows = pl.ds(pl.multiple_of(yy * 32, 32), 32)
        return part[s, j, 0, rows, :] + dsum[s, j, rows, :]

    def do_y1(s, g):
        pair = (2 * g, 2 * g + 1)
        for j in pair:
            c_d(s, j).wait_recv()
        for i, j in enumerate(pair):
            y1s[s, g, 0, i] = own(s, j, y1 if g == 0 else y3).astype(BF16)
            y1s[s, g, 1, i] = own(s, j, y2).astype(BF16)
        c_y1(s, g).start()

    def do_y2(s, g):
        c_y1(s, g).wait_recv()
        for i, j in enumerate((2 * g, 2 * g + 1)):
            y2s[s, g, i] = own(s, j, y3 if g == 0 else y1) + y1r[s, g, 1, i].astype(F32)
        c_y2(s, g).start()

    def do_x(s, g):
        c_y2(s, g).wait_recv()
        for i, j in enumerate((2 * g, 2 * g + 1)):
            xs[s, j] = own(s, j, y) + y1r[s, g, 0, i].astype(F32) + y2r[s, g, i]
            if j > 0:
                c_x(s, j).start()

    def do_z(s):
        for j in (1, 2, 3):
            c_x(s, j).wait_recv()
        zs[s] = xs[s, 0] + xr[s, 1] + xr[s, 2] + xr[s, 3]

        @pl.when(s > 0)
        def _():
            c_z(s).start()

    def visit(t, carry):
        def at(offset, act):
            s = (t - offset + 16) // 4 - 4

            @pl.when(((t - offset + 16) % 4 == 0) & (s >= 0) & (s <= zp))
            def _():
                act(s)

        def act_a(s):
            @pl.when(s > 0)
            def _():
                c_kzr(s).wait_recv()
                pass_on(s)

        def act_b(s):
            c_kx(s, 1).wait_recv()
            c_kx(s, 2).wait_recv()
            c_kh(s, 0).start()
            c_kh(s, 1).start()
            c_kd(s, 1).start()
            c_kd(s, 2).start()

        def act_c(s):
            c_kh(s, 0).wait_recv()
            c_kh(s, 1).wait_recv()
            c_kd(s, 3).start()

        at(0, act_b)
        at(-4, act_a)
        at(2, act_c)
        at(13, do_z)
        at(11, lambda s: do_x(s, 1))
        at(9, lambda s: do_x(s, 0))
        at(8, lambda s: do_y2(s, 1))
        at(6, lambda s: do_y2(s, 0))
        at(5, lambda s: do_y1(s, 1))
        at(3, lambda s: do_y1(s, 0))

        @pl.when(t < 4 * zp + 4)
        def _():
            s, j = t // 4, t % 4
            c_kd(s, j).wait_recv()
            tile(s, j)
            c_d(s, j).start()

        over = t - (4 * zp + 4)

        @pl.when(over == 0)
        def _():
            low[...] = mix[0:512, :].astype(BF16)
            for rel in (1, 0):
                half = c if rel == 0 else 1 - c
                for hh in (0, 1):
                    cols = pl.ds(pl.multiple_of((2 * half + hh) * 128, 128), 128)
                    got = factor * dot(low[:, cols], qm[:, cols])
                    term[rel, :, :, :, hh * 128 : (hh + 1) * 128] = got.reshape(16, 4, 8, 128)
                if rel == 1:
                    c_t.start()

        @pl.when(over == 1)
        def _():
            c_t.wait_recv()
            for j in range(4):
                turn = (x, x1, x3, x2)[j]
                got = (term[0, :, turn] + termr[:, turn]).reshape(128, 256)
                if j == 0:
                    wx0[...] = got
                else:
                    wxs[j] = got.astype(BF16)
                    c_wx(j).start()
            for h in range(4):
                cols = pl.ds(h * 128, 128)
                o_main[:, cols] = factor * dot(low[:, cols], kw[:, cols], TN)
            for g in range(2):
                a = mix[512:640, pl.ds(g * 256, 128)].T
                b = mix[512:640, pl.ds(g * 256 + 128, 128)].T
                o_rot[:, pl.ds(g * 128, 128)] = factor * jnp.concatenate([a[:, 0:64], b[:, 0:64]], axis=1)

        @pl.when(over == 3)
        def _():
            got = wx0[...]
            for j in (1, 2, 3):
                c_wx(j).wait_recv()
                got = got + wxr[j].astype(F32)
            wz[...] = got.reshape(16, 8, 256)

            def go(d, carry):
                c_wz(d).start()
                return carry

            lax.fori_loop(1, 16, go, 0)

        return carry

    lax.fori_loop(0, 4 * zp + 14, visit, 0)

    def wait_z(d, carry):
        c_zr(d).wait_recv()
        zs[0] += zr[d]
        return carry

    lax.fori_loop(1, more + 1, wait_z, 0)
    fin[0] = zs[0]
    for j in (1, 2, 3):
        c_f(j).start()

    def wait_wz(d, total):
        c_wz(d).wait_recv()
        return total + wzr[d]

    wf[...] = lax.fori_loop(1, 16, wait_wz, wz[z])
    c_wf.start()

    for j in range(4):
        if j > 0:
            c_f(j).wait_recv()
        rows = pl.ds(pl.multiple_of((y, y1, y3, y2)[j] * 32, 32), 32)
        o_lat[rows, :] = fin[j, :, 0:512]
        o_krot[rows, :] = fin[j, :, 512:576]
    c_wf.wait_recv()

    @pl.when(c == 0)
    def _():
        o_weight[:, 0:256] = wf[0:4, :]
        o_weight[:, 256:512] = wfr[0:4, :]

    @pl.when(c == 1)
    def _():
        o_weight[:, 0:256] = wfr[4:8, :]
        o_weight[:, 256:512] = wf[4:8, :]

    def drain(s, carry):
        @pl.when(more > 0)
        def _():
            c_kz(s).wait_send()

        for j in (1, 2):
            c_kx(s, j).wait_send()
        for j in (0, 1):
            c_kh(s, j).wait_send()
            c_y1(s, j).wait_send()
            c_y2(s, j).wait_send()
        for j in range(4):
            c_kd(s, j).wait_send()
            c_d(s, j).wait_send()
            if j > 0:
                c_x(s, j).wait_send()

        @pl.when(s > 0)
        def _():
            c_z(s).wait_send()

        return carry

    lax.fori_loop(0, zp + 1, drain, 0)
    c_t.wait_send()
    c_wf.wait_send()
    for j in (1, 2, 3):
        c_wx(j).wait_send()
        c_f(j).wait_send()

    def drain_wz(d, carry):
        c_wz(d).wait_send()
        return carry

    lax.fori_loop(1, 16, drain_wz, 0)


def per_device(query_main, query_rotary, latent, key_rotary, key_weight, value_weight, head_output, output_grad, row_logsum):
    kcat = jnp.concatenate([latent, key_rotary, jnp.zeros((128, 64), BF16)], axis=1)
    v = pl.BlockSpec(memory_space=pltpu.VMEM)
    hbm = pl.BlockSpec(memory_space=pl.ANY)
    dma = pltpu.SemaphoreType.DMA
    scratch = [
        pltpu.VMEM((5, 4, 2, 128, WIDE), BF16),
        pltpu.VMEM((4, 4, 2, 128, WIDE), F32),
        pltpu.VMEM((4, 4, 128, WIDE), F32),
        pltpu.VMEM((4, 2, 2, 2, 32, WIDE), BF16),
        pltpu.VMEM((4, 2, 2, 2, 32, WIDE), BF16),
        pltpu.VMEM((4, 2, 2, 32, WIDE), F32),
        pltpu.VMEM((4, 2, 2, 32, WIDE), F32),
        pltpu.VMEM((4, 4, 32, WIDE), F32),
        pltpu.VMEM((4, 4, 32, WIDE), F32),
        pltpu.VMEM((4, 32, WIDE), F32),
        pltpu.VMEM((4, 32, WIDE), F32),
        pltpu.VMEM((4, 32, WIDE), F32),
        pltpu.VMEM((WIDE, 512), F32),
        pltpu.VMEM((512, WIDE), BF16),
        pltpu.VMEM((512, 512), BF16),
        pltpu.VMEM((8, 512), F32),
        pltpu.VMEM((512, 512), BF16),
        pltpu.VMEM((2, 16, 4, 8, 256), F32),
        pltpu.VMEM((16, 4, 8, 256), F32),
        pltpu.VMEM((128, 256), F32),
        pltpu.VMEM((4, 128, 256), BF16),
        pltpu.VMEM((4, 128, 256), BF16),
        pltpu.VMEM((16, 8, 256), F32),
        pltpu.VMEM((16, 8, 256), F32),
        pltpu.VMEM((8, 256), F32),
        pltpu.VMEM((8, 256), F32),
        dma,
        dma((5,)), dma((5,)),
        dma((4, 4)), dma((4, 4)),
        dma((4, 4)), dma((4, 4)),
        dma((4, 4)), dma((4, 4)),
        dma((4, 2)), dma((4, 2)),
        dma((4, 2)), dma((4, 2)),
        dma((4, 4)), dma((4, 4)),
        dma((4,)), dma((4,)),
        dma((4,)), dma((4,)),
        dma, dma,
        dma((4,)), dma((4,)),
        dma((16,)), dma((16,)),
        dma, dma,
    ]
    return pl.pallas_call(
        body,
        out_shape=(
            jax.ShapeDtypeStruct((128, 512), F32),
            jax.ShapeDtypeStruct((128, 256), F32),
            jax.ShapeDtypeStruct((128, 512), F32),
            jax.ShapeDtypeStruct((128, 64), F32),
            jax.ShapeDtypeStruct((4, 512), F32),
        ),
        in_specs=[v, v, hbm, v, v, v, v, v],
        out_specs=(v,) * 5,
        scratch_shapes=scratch,
        compiler_params=pltpu.CompilerParams(
            collective_id=0, has_side_effects=True, vmem_limit_bytes=60 * 1024 * 1024
        ),
    )(query_main, query_rotary, kcat, key_weight, value_weight, head_output, output_grad, row_logsum)


def solution(mesh):
    finer = Mesh(mesh.devices.reshape(16, 4, 2, mesh.shape["tp"]), ("z", "x", "c", "y"))
    return jax.shard_map(
        per_device,
        mesh=finer,
        in_specs=(
            P(SP, "y"),
            P(SP, "y"),
            P(SP, None),
            P(SP, None),
            P(None, "y"),
            P(None, "y"),
            P(SP, "y"),
            P(SP, "y"),
            P("y", SP),
        ),
        out_specs=(P(SP, "y"), P(SP, "y"), P(SP, None), P(SP, None), P(SP, "y")),
        check_vma=False,
    )
```

time: 744 us -> 95.4 us (0.13)
  the two profiles are of different devices: /device:TPU:8 before, /device:TPU:96 now
where the time goes in v1:
time: 95.4 us; the launch traced here: 95 us
  Pallas kernels  86.3 us (90%)
  local copies, waits for them, and re-layouts  6.45 us (7%)
  other arithmetic  1.61 us (2%)
    pallas_call x1, Pallas kernels, per_device(): pl.pallas_call(body, out_shape=(jax.ShapeDtypeStruct((128, 512), F32), ja...  86.3 us
    unnamed x11, local copies, waits for them, and re-layouts  4.83 us

profile of v1, /device:TPU:96, one launch (start us, length us, event | category | flops | bytes accessed | tf_op | source)
XLA Modules:
  0.0 95.0 jit_solution(5990681478890274357)
XLA Ops:
  0.6 0.1 pad.2.clone
  0.7 0.8 copy.14
  1.5 1.6 %maximum_maximum_fusion.kcat = bf16[128,640]{1,0:T(8,128)(2,1)} fusion(bf16[128,64]{1,0:T(8,128)(2,1)S(1)} %copy.14, bf16[128,512]{1,0:T(8,128)(2,1)} %param.11, bf16[640]{0:T(1024)(128)(2,1)S(1)} %pad.2.clone), kind=kLoop, calls=%fused_computation | loop fusion | flops 491520 | bytes 312576 | tf_op jit(solution)/shard_map/concatenate | solution.py:369
  3.2 86.3 %shard_map.128 = (f32[128,512]{1,0:T(8,128)}, f32[128,256]{1,0:T(8,128)}, f32[128,512]{1,0:T(8,128)}, f32[128,64]{1,0:T(8,128)}, f32[4,512]{1,0:T(4,128)}) custom-call(bf16[128,512]{1,0:T(8,128)(2,1)} %qm.1, bf16[128,256]{1,0:T(8,128)(2,1)} %qr.1, bf16[128,640]{1,0:T(8,128)(2,1)} %maximum_maximum_fusion.kcat, bf16[512,512]{1,0:T(8,128)(2,1)} %kw.1, ...), custom_call_target="tpu_custom_call" | custom-call | tf_op jit(solution)/shard_map/pallas_call | solution.py:415
  89.5 1.5 %copy.15 = f32[128,64]{0,1:T(8,128)} copy(f32[128,64]{1,0:T(8,128)} %get-tuple-element.8) | data formatting | bytes 65536 | tf_op jit(solution)/shard_map/pallas_call | solution.py:415
  91.0 0.0 copy-start.1
  91.0 1.7 %copy.20 = f32[128,512]{1,0:T(8,128)} copy(f32[128,512]{1,0:T(8,128)} %get-tuple-element.15) | data formatting | bytes 524288
  92.7 0.0 copy-done.1
  92.7 0.0 copy-start
  92.7 0.7 copy.21
  93.4 0.3 copy-done
  93.7 0.0 copy-start.2
  93.7 0.7 copy.22
  94.4 0.0 copy-done.2
  94.4 0.6 copy.23
  (1 shorter events, 0.0 us)
Async XLA Ops:
  91.0 1.7 %copy-start.1 = (f32[128,256]{1,0:T(8,128)S(1)}, f32[128,256]{1,0:T(8,128)}, u32[]{:S(2)}) copy-start(f32[128,256]{1,0:T(8,128)} %get-tuple-element.16) | copy-start | bytes 393220
  92.7 1.0 %copy-start = (f32[128,512]{1,0:T(8,128)S(1)}, f32[128,512]{1,0:T(8,128)}, u32[]{:S(2)}) copy-start(f32[128,512]{1,0:T(8,128)} %get-tuple-element.17) | copy-start | bytes 786436
  93.7 0.7 copy-start.2

commit v2 on v1

v2 whole, which is shorter than its diff:
```python
import jax
import jax.numpy as jnp
from jax import lax
from jax.experimental import pallas as pl
from jax.experimental.pallas import tpu as pltpu
from jax.sharding import Mesh
from jax.sharding import PartitionSpec as P

MESH = pl.DeviceIdType.MESH
SP = ("z", "x", "c")
F32 = jnp.float32
BF16 = jnp.bfloat16
WIDE = 640
NT = (((1,), (1,)), ((), ()))
TN = (((0,), (0,)), ((), ()))


def dot(a, b, dims=(((1,), (0,)), ((), ()))):
    return lax.dot_general(a, b, dims, preferred_element_type=F32)


ORDER_S = (0, 1, 0, 0, 1, 1, 2, 2, 2, 0, 1, 2, 3, 3, 3, 3)
ORDER_J = (0, 0, 1, 2, 1, 2, 0, 1, 2, 3, 3, 3, 3, 1, 2, 0)


def pick(table, t):
    out = jnp.int32(0)
    for k, v in enumerate(table):
        if v:
            out = out + jnp.where(t == k, v, 0)
    return out


def body(
    qm, qr, lat, krt, kw, vw, ho, og, ls,
    o_main, o_rot, o_lat, o_krot, o_weight,
    qb, st, qc, gr, keys, mix, part, dsum, y1s, y1r, y2s, y2r, zs, zr, fin,
    dqs, dqh, dqr, term, termr, wx0, wxs, wxr, wz, wzr, wf, wfr,
    s_loc, s_q, r_q, s_st, r_st, s_kz, r_kz, s_kd, r_kd, s_d, r_d, s_y1, r_y1, s_y2, r_y2,
    s_z, r_z, s_f, r_f, s_dh, r_dh, s_dq, r_dq, s_t, r_t, s_wx, r_wx, s_wz, r_wz, s_wf, r_wf,
):
    z, x, c, y = (lax.axis_index(a) for a in ("z", "x", "c", "y"))
    factor = 192.0 ** (-0.5)
    zp = jnp.where(z < 3, z, (z + 1) % 4)
    planes = jnp.where(z < 3, 3, jnp.where(z < 15, 4, 1))
    more = planes - 1 - zp
    sib = {"c": 1 - c}
    x1, x3, x2 = x + 1 - 2 * (x % 2), 3 - x, (x + 2) % 4
    y1, y3, y2 = y + 1 - 2 * (y % 2), 3 - y, (y + 2) % 4
    xdev = (None, {"x": x1}, {"x": x3}, {"x": x2})
    ydev = (None, {"y": y1}, {"y": y3}, {"y": y2})

    def remote(src, dst, ss, rs, dev):
        return pltpu.make_async_remote_copy(
            src_ref=src, dst_ref=dst, send_sem=ss, recv_sem=rs, device_id=dev, device_id_type=MESH
        )

    def c_q(j):
        return remote(qb.at[0], qb.at[j], s_q.at[j], r_q.at[j], xdev[j])

    def c_qh(i):
        rows = pl.ds(64 * i, 64)
        return remote(qb.at[1 + i, rows], qb.at[3, rows], s_q.at[3 + i], r_q.at[3 + i], xdev[2 - i])

    def c_st(j):
        return remote(st.at[0], st.at[j], s_st.at[j], r_st.at[j], xdev[j])

    def c_kz(s):
        return remote(keys.at[s, 0], keys.at[s + 1, 0], s_kz.at[s], r_kz.at[s + 1], {"z": z + 1})

    def c_kzr(s):
        return remote(keys.at[s, 0], keys.at[s, 0], s_kz.at[s], r_kz.at[s], {"z": z - 1})

    def c_kd(s):
        return remote(keys.at[s, 0], keys.at[s, 1], s_kd.at[s], r_kd.at[s], sib)

    def c_d(s):
        return remote(part.at[s, 1], dsum.at[s], s_d.at[s], r_d.at[s], sib)

    def c_y1(s, g):
        return remote(y1s.at[s, g], y1r.at[s, g], s_y1.at[s, g], r_y1.at[s, g], ydev[1 + g])

    def c_y2(s, g):
        return remote(y2s.at[s, g], y2r.at[s, g], s_y2.at[s, g], r_y2.at[s, g], ydev[2 - g])

    def c_z(s):
        return remote(zs.at[s], zr.at[s], s_z.at[s], r_z.at[s], {"z": z - s})

    def c_zr(s):
        return remote(zs.at[s], zr.at[s], s_z.at[s], r_z.at[s], {"z": z + s})

    def c_f(j):
        return remote(fin.at[0], fin.at[j], s_f.at[j], r_f.at[j], ydev[j])

    def c_dh(i):
        rows = pl.ds(64 * i, 64)
        return remote(dqs.at[3, rows], dqh.at[i], s_dh.at[i], r_dh.at[i], xdev[1 + i])

    def c_dq(j):
        return remote(dqs.at[j], dqr.at[j - 1], s_dq.at[j], r_dq.at[j], xdev[j])

    c_t = remote(term.at[1], termr, s_t, r_t, sib)

    def c_wx(j):
        return remote(wxs.at[j], wxr.at[j], s_wx.at[j], r_wx.at[j], xdev[j])

    def c_wz(d):
        to = (z + d) % 16
        return remote(wz.at[to], wzr.at[d], s_wz.at[d], r_wz.at[d], {"z": to})

    c_wf = remote(wf, wfr, s_wf, r_wf, sib)

    loads = [
        pltpu.make_async_copy(qm, qb.at[0, :, 0:512], s_loc.at[0]),
        pltpu.make_async_copy(qr, qb.at[0, :, 512:768], s_loc.at[1]),
        pltpu.make_async_copy(og, qb.at[0, :, 768:1280], s_loc.at[2]),
        pltpu.make_async_copy(lat, keys.at[0, 0, :, 0:512], s_loc.at[3]),
    ]
    for copy in loads:
        copy.start()
    barrier = pltpu.get_barrier_semaphore()
    for dev in (sib, *xdev[1:], *ydev[1:]):
        pl.semaphore_signal(barrier, inc=1, device_id=dev, device_id_type=MESH)

    def greet(d, carry):
        pl.semaphore_signal(barrier, inc=1, device_id={"z": (z + d) % 16}, device_id_type=MESH)
        return carry

    lax.fori_loop(1, 16, greet, 0)
    keys[0, 0, :, 512:WIDE] = jnp.concatenate([krt[...].T, jnp.zeros((128, 64), BF16)], axis=1)
    for copy in loads:
        copy.wait()
    pl.semaphore_wait(barrier, 22)

    def pass_on(s):
        @pl.when(more > 0)
        def _():
            c_kz(s).start()

        c_kd(s).start()

    c_q(1).start()
    c_q(2).start()
    pass_on(0)

    ones = jnp.ones((8, 128), F32)
    for h in range(4):
        cols = pl.ds(h * 128, 128)
        prod = ho[:, cols].astype(F32) * qb[0, :, 768 + h * 128 : 896 + h * 128].astype(F32)
        sums = lax.dot_general(
            ones, prod, NT, precision=lax.Precision.HIGHEST, preferred_element_type=F32
        )
        st[0, 1:2, cols] = sums[0:1, :]
        st[0, 0:1, cols] = ls[h : h + 1, :]
    for j in (1, 2, 3):
        c_st(j).start()

    def project(j):
        for h in range(4):
            cols = pl.ds(h * 128, 128)
            rows = pl.ds(h * 128, 128)
            qc[j, rows, 0:512] = dot(qb[j, :, h * 128 : h * 128 + 128], kw[:, cols], NT).astype(BF16)
            gr[j, rows, :] = dot(qb[j, :, 768 + h * 128 : 896 + h * 128], vw[:, cols], NT).astype(BF16)
            rot = qb[j, :, 512 + h * 64 : 576 + h * 64]
            qc[j, rows, 512:WIDE] = jnp.concatenate([rot, jnp.zeros((128, 64), BF16)], axis=1)

    project(0)
    mix[...] = jnp.zeros_like(mix)
    part[...] = jnp.zeros_like(part)

    def tile(s, j):
        kt = keys[s].reshape(256, WIDE)
        turn = jnp.where(j == 0, x, jnp.where(j == 1, x1, jnp.where(j == 2, x3, x2)))
        far = jnp.where(s > 0, 1 << 20, 0)
        first = (2 * x + c) * 128 - far
        second = (2 * x + 1 - c) * 128 - 128 - far
        k_row = lax.broadcasted_iota(jnp.int32, (256, 1), 0)
        k_place = jnp.where(k_row < 128, k_row + first, k_row + second)
        q_place = lax.broadcasted_iota(jnp.int32, (1, 512), 1) % 128 + (2 * turn + c) * 128
        scores = dot(kt, qc[j], NT)
        weights = jnp.where(k_place <= q_place, jnp.exp(factor * scores - st[j, 0:1, :]), 0.0)
        slopes = dot(kt[:, 0:512], gr[j], NT)
        dscores = weights * (slopes - st[j, 1:2, :])
        w_low = weights.astype(BF16)
        d_low = dscores.astype(BF16)
        mix[j] += dot(kt, d_low, TN)
        main = factor * dot(d_low, qc[j, :, 0:512]) + dot(w_low, gr[j])
        rest = factor * dot(d_low, qc[j, :, 512:WIDE])
        part[s, :, :, 0:512] += main.reshape(2, 128, 512)
        part[s, :, :, 512:WIDE] += rest.reshape(2, 128, 128)

    def own(s, g, yy):
        rows = pl.ds(pl.multiple_of(yy * 32 + 16 * g, 16), 16)
        return part[s, 0, rows, :] + dsum[s, rows, :]

    def do_y1(s):
        c_d(s).wait_recv()
        for g in (0, 1):
            y1s[s, g, 0] = own(s, g, (y1, y3)[g])
            y1s[s, g, 1] = own(s, g, y2)
            c_y1(s, g).start()

    def do_y2(s):
        for g in (0, 1):
            c_y1(s, g).wait_recv()
            y2s[s, g] = own(s, g, (y3, y1)[g]) + y1r[s, g, 1]
            c_y2(s, g).start()

    def do_z(s):
        for g in (0, 1):
            c_y2(s, g).wait_recv()
            zs[s, 16 * g : 16 * g + 16, :] = own(s, g, y) + y1r[s, g, 0] + y2r[s, g]

        @pl.when(s > 0)
        def _():
            c_z(s).start()

    def each(act, last=3):
        def step(s, carry):
            act(s)
            return carry

        lax.fori_loop(0, jnp.minimum(zp, last) + 1, step, 0)

    def do_dq(j):
        for h in range(4):
            cols = pl.ds(h * 128, 128)
            m = mix[j, 0:512, cols]
            high = m.astype(BF16)
            rest = (m - high.astype(F32)).astype(BF16)
            got = dot(high, kw[:, cols], TN) + dot(rest, kw[:, cols], TN)
            dqs[j, :, cols] = factor * got
        for g in range(2):
            a = mix[j, 512:640, g * 256 : g * 256 + 128].T
            b = mix[j, 512:640, g * 256 + 128 : g * 256 + 256].T
            dqs[j, :, 512 + g * 128 : 640 + g * 128] = factor * jnp.concatenate(
                [a[:, 0:64], b[:, 0:64]], axis=1
            )

    def visit(t, carry):
        s, j = pick(ORDER_S, t), pick(ORDER_J, t)

        def arrive(k):
            @pl.when((t == {1: 1, 2: 4, 3: 12}[k]) & (zp >= k))
            def _():
                c_kzr(k).wait_recv()
                pass_on(k)

        arrive(1)
        arrive(2)
        arrive(3)

        @pl.when(((t < 2) | (t == 6) | (t == 12)) & (s <= zp))
        def _():
            c_kd(s).wait_recv()

        @pl.when(t == 2)
        def _():
            c_q(1).wait_recv()
            c_q(2).wait_recv()
            c_qh(0).start()
            c_qh(1).start()
            for k in (1, 2):
                c_st(k).wait_recv()
                project(k)

        @pl.when(t == 9)
        def _():
            c_qh(0).wait_recv()
            c_qh(1).wait_recv()
            c_st(3).wait_recv()
            project(3)

        @pl.when(t == 12)
        def _():
            each(lambda s: c_d(s).start(), 2)

        @pl.when(t == 14)
        def _():
            each(do_y1, 2)

        @pl.when(s <= zp)
        def _():
            tile(s, j)

        @pl.when(t == 12)
        def _():
            do_dq(3)
            c_dh(0).start()
            c_dh(1).start()

        return carry

    lax.fori_loop(0, 16, visit, 0)

    @pl.when(zp == 3)
    def _():
        c_d(3).start()

    for rel in (1, 0):
        half = c if rel == 0 else 1 - c
        for hh in (0, 1):
            cols = pl.ds(pl.multiple_of((2 * half + hh) * 128, 128), 128)
            got = jnp.zeros((512, 128), F32)
            for j in range(4):
                m = mix[j, 0:512, cols]
                high = m.astype(BF16)
                rest = (m - high.astype(F32)).astype(BF16)
                q = qb[j, :, cols]
                got = got + dot(jnp.concatenate([high, rest], axis=1), jnp.concatenate([q, q], axis=0))
            term[rel, :, :, :, hh * 128 : (hh + 1) * 128] = (factor * got).reshape(16, 4, 8, 128)
        if rel == 1:
            c_t.start()
    each(do_y2, 2)
    c_t.wait_recv()
    for j in range(4):
        turn = (x, x1, x3, x2)[j]
        got = (term[0, :, turn] + termr[:, turn]).reshape(128, 256)
        if j == 0:
            wx0[...] = got
        else:
            wxs[j] = got.astype(BF16)
            c_wx(j).start()

    do_dq(1)
    c_dh(1).wait_recv()
    dqs[1, 64:128, :] += dqh[1]
    c_dq(1).start()
    do_dq(2)
    c_dh(0).wait_recv()
    dqs[2, 0:64, :] += dqh[0]
    c_dq(2).start()

    @pl.when(zp == 3)
    def _():
        do_y1(3)

    each(do_z, 2)
    got = wx0[...]
    for j in (1, 2, 3):
        c_wx(j).wait_recv()
        got = got + wxr[j].astype(F32)
    wz[...] = got.reshape(16, 8, 256)

    def go(d, carry):
        c_wz(d).start()
        return carry

    lax.fori_loop(1, 16, go, 0)

    @pl.when(zp == 3)
    def _():
        do_y2(3)

    do_dq(0)

    @pl.when(zp == 3)
    def _():
        do_z(3)

    def wait_z(d, carry):
        c_zr(d).wait_recv()
        zs[0] += zr[d]
        return carry

    lax.fori_loop(1, more + 1, wait_z, 0)
    fin[0] = zs[0]
    for j in (1, 2, 3):
        c_f(j).start()

    def wait_wz(d, total):
        c_wz(d).wait_recv()
        return total + wzr[d]

    wf[...] = lax.fori_loop(1, 16, wait_wz, wz[z])
    c_wf.start()

    c_dq(1).wait_recv()
    c_dq(2).wait_recv()
    o_main[...] = dqs[0, :, 0:512] + dqr[0, :, 0:512] + dqr[1, :, 0:512]
    o_rot[...] = dqs[0, :, 512:768] + dqr[0, :, 512:768] + dqr[1, :, 512:768]

    for j in range(4):
        if j > 0:
            c_f(j).wait_recv()
        rows = pl.ds(pl.multiple_of((y, y1, y3, y2)[j] * 32, 32), 32)
        o_lat[rows, :] = fin[j, :, 0:512]
        o_krot[rows, :] = fin[j, :, 512:640]
    c_wf.wait_recv()

    @pl.when(c == 0)
    def _():
        o_weight[:, 0:256] = wf[0:4, :]
        o_weight[:, 256:512] = wfr[0:4, :]

    @pl.when(c == 1)
    def _():
        o_weight[:, 0:256] = wfr[4:8, :]
        o_weight[:, 256:512] = wf[4:8, :]

    def drain(s):
        @pl.when(more > 0)
        def _():
            c_kz(s).wait_send()

        c_kd(s).wait_send()
        c_d(s).wait_send()
        for g in (0, 1):
            c_y1(s, g).wait_send()
            c_y2(s, g).wait_send()

        @pl.when(s > 0)
        def _():
            c_z(s).wait_send()

    each(drain)
    c_t.wait_send()
    c_wf.wait_send()
    for i in (0, 1):
        c_q(1 + i).wait_send()
        c_qh(i).wait_send()
        c_dh(i).wait_send()
        c_dq(1 + i).wait_send()
    for j in (1, 2, 3):
        c_st(j).wait_send()
        c_wx(j).wait_send()
        c_f(j).wait_send()

    def drain_wz(d, carry):
        c_wz(d).wait_send()
        return carry

    lax.fori_loop(1, 16, drain_wz, 0)


def put_out(a, b, d, e, f, oa, ob, od, oe, of):
    oa[...] = a[...]
    ob[...] = b[...]
    od[...] = d[...]
    oe[...] = e[...].T[0:64, :]
    of[...] = f[...]


def per_device(query_main, query_rotary, latent, key_rotary, key_weight, value_weight, head_output, output_grad, row_logsum):
    v = pl.BlockSpec(memory_space=pltpu.VMEM)
    hbm = pl.BlockSpec(memory_space=pl.ANY)
    dma = pltpu.SemaphoreType.DMA
    scratch = [
        pltpu.VMEM((4, 128, 1280), BF16),
        pltpu.VMEM((4, 8, 512), F32),
        pltpu.VMEM((4, 512, WIDE), BF16),
        pltpu.VMEM((4, 512, 512), BF16),
        pltpu.VMEM((4, 2, 128, WIDE), BF16),
        pltpu.VMEM((4, WIDE, 512), F32),
        pltpu.VMEM((4, 2, 128, WIDE), F32),
        pltpu.VMEM((4, 128, WIDE), F32),
        pltpu.VMEM((4, 2, 2, 16, WIDE), F32),
        pltpu.VMEM((4, 2, 2, 16, WIDE), F32),
        pltpu.VMEM((4, 2, 16, WIDE), F32),
        pltpu.VMEM((4, 2, 16, WIDE), F32),
        pltpu.VMEM((4, 32, WIDE), F32),
        pltpu.VMEM((4, 32, WIDE), F32),
        pltpu.VMEM((4, 32, WIDE), F32),
        pltpu.VMEM((4, 128, 768), F32),
        pltpu.VMEM((2, 64, 768), F32),
        pltpu.VMEM((2, 128, 768), F32),
        pltpu.VMEM((2, 16, 4, 8, 256), F32),
        pltpu.VMEM((16, 4, 8, 256), F32),
        pltpu.VMEM((128, 256), F32),
        pltpu.VMEM((4, 128, 256), BF16),
        pltpu.VMEM((4, 128, 256), BF16),
        pltpu.VMEM((16, 8, 256), F32),
        pltpu.VMEM((16, 8, 256), F32),
        pltpu.VMEM((8, 256), F32),
        pltpu.VMEM((8, 256), F32),
        dma((4,)),
        dma((5,)), dma((5,)),
        dma((4,)), dma((4,)),
        dma((4,)), dma((5,)),
        dma((4,)), dma((4,)),
        dma((4,)), dma((4,)),
        dma((4, 2)), dma((4, 2)),
        dma((4, 2)), dma((4, 2)),
        dma((4,)), dma((4,)),
        dma((4,)), dma((4,)),
        dma((2,)), dma((2,)),
        dma((3,)), dma((3,)),
        dma, dma,
        dma((4,)), dma((4,)),
        dma((16,)), dma((16,)),
        dma, dma,
    ]
    got = pl.pallas_call(
        body,
        out_shape=(
            jax.ShapeDtypeStruct((128, 512), F32),
            jax.ShapeDtypeStruct((128, 256), F32),
            jax.ShapeDtypeStruct((128, 512), F32),
            jax.ShapeDtypeStruct((128, 128), F32),
            jax.ShapeDtypeStruct((4, 512), F32),
        ),
        in_specs=[hbm, hbm, hbm, v, v, v, v, hbm, v],
        out_specs=(v,) * 5,
        scratch_shapes=scratch,
        compiler_params=pltpu.CompilerParams(
            collective_id=0, has_side_effects=True, vmem_limit_bytes=56 * 1024 * 1024
        ),
    )(query_main, query_rotary, latent, key_rotary.T, key_weight, value_weight, head_output, output_grad, row_logsum)
    main, rot, lat, krot, weight = pl.pallas_call(
        put_out,
        out_shape=(
            jax.ShapeDtypeStruct((128, 512), F32),
            jax.ShapeDtypeStruct((128, 256), F32),
            jax.ShapeDtypeStruct((128, 512), F32),
            jax.ShapeDtypeStruct((64, 128), F32),
            jax.ShapeDtypeStruct((4, 512), F32),
        ),
        in_specs=[v] * 5,
        out_specs=(v,) * 5,
    )(*got)
    return main, rot, lat, krot.T, weight


def solution(mesh):
    finer = Mesh(mesh.devices.reshape(16, 4, 2, mesh.shape["tp"]), ("z", "x", "c", "y"))
    return jax.shard_map(
        per_device,
        mesh=finer,
        in_specs=(
            P(SP, "y"),
            P(SP, "y"),
            P(SP, None),
            P(SP, None),
            P(None, "y"),
            P(None, "y"),
            P(SP, "y"),
            P(SP, "y"),
            P("y", SP),
        ),
        out_specs=(P(SP, "y"), P(SP, "y"), P(SP, None), P(SP, None), P(SP, "y")),
        check_vma=False,
    )
```

time: 95.4 us -> 76.3 us (0.80)
  the two profiles are of different devices: /device:TPU:96 before, /device:TPU:97 now
where the time goes in v2:
time: 76.3 us; the launch traced here: 76.1 us
  Pallas kernels  75.4 us (99%)
    pallas_call x1, Pallas kernels, per_device(): pl.pallas_call(body, out_shape=(jax.ShapeDtypeStruct((128, 512), F32), ja...  73.5 us
    pallas_call x1, Pallas kernels, per_device(): pl.pallas_call(put_out, out_shape=(jax.ShapeDtypeStruct((128, 512), F32),...  1.98 us

profile of v2, /device:TPU:97, one launch (start us, length us, event | category | flops | bytes accessed | tf_op | source)
XLA Modules:
  0.0 76.1 jit_solution(15383600249733615644)
XLA Ops:
  0.6 73.5 %shard_map.128 = (f32[128,512]{1,0:T(8,128)}, f32[128,256]{1,0:T(8,128)}, f32[128,512]{1,0:T(8,128)}, f32[128,128]{1,0:T(8,128)}, f32[4,512]{1,0:T(4,128)}) custom-call(bf16[128,512]{1,0:T(8,128)(2,1)} %qm.1, bf16[128,256]{1,0:T(8,128)(2,1)} %qr.1, bf16[128,512]{1,0:T(8,128)(2,1)} %lat.1, bf16[64,128]{1,0:T(8,128)(2,1)} %bitcast.2, bf16[512,512]{1,0:T(8,128)(2,1)} %kw.1, ...), custom_call_target="tpu_custom_call" | custom-call | tf_op jit(solution)/shard_map/pallas_call | solution.py:493
  74.1 2.0 %shard_map.129 = (f32[128,512]{1,0:T(8,128)}, f32[128,256]{1,0:T(8,128)}, f32[128,512]{1,0:T(8,128)}, f32[64,128]{1,0:T(8,128)}, f32[4,512]{1,0:T(4,128)}) custom-call(f32[128,512]{1,0:T(8,128)} %get-tuple-element.15.a, f32[128,256]{1,0:T(8,128)} %get-tuple-element.16.b, f32[128,512]{1,0:T(8,128)} %get-tuple-element.17.d, f32[128,128]{1,0:T(8,128)} %get-tuple-element.18.e, ...), custom_call_target="tpu_custom_call" | custom-call | tf_op jit(solution)/shard_map/pallas_call | solution.py:509

commit v3 on v2

--- a/solution.py
+++ b/solution.py
@@ -19,10 +19,6 @@
     return lax.dot_general(a, b, dims, preferred_element_type=F32)
 
 
-ORDER_S = (0, 1, 0, 0, 1, 1, 2, 2, 2, 0, 1, 2, 3, 3, 3, 3)
-ORDER_J = (0, 0, 1, 2, 1, 2, 0, 1, 2, 3, 3, 3, 3, 1, 2, 0)
-
-
 def pick(table, t):
     out = jnp.int32(0)
     for k, v in enumerate(table):
@@ -32,11 +28,11 @@
 
 
 def body(
-    qm, qr, lat, krt, kw, vw, ho, og, ls,
+    qm, qr, lat, krt, kwh, vwh, hoh, og, lsh,
     o_main, o_rot, o_lat, o_krot, o_weight,
-    qb, st, qc, gr, keys, mix, part, dsum, y1s, y1r, y2s, y2r, zs, zr, fin,
+    kw, vw, ho, ls, krv, qb, st, sts, qc, gr, keys, mix, part, dsum, y1s, y1r, y2s, y2r, zs, zr, fin,
     dqs, dqh, dqr, term, termr, wx0, wxs, wxr, wz, wzr, wf, wfr,
-    s_loc, s_q, r_q, s_st, r_st, s_kz, r_kz, s_kd, r_kd, s_d, r_d, s_y1, r_y1, s_y2, r_y2,
+    s_loc, s_out, hop, s_q, r_q, s_st, r_st, s_kz, r_kz, s_kd, r_kd, s_d, r_d, s_y1, r_y1, s_y2, r_y2,
     s_z, r_z, s_f, r_f, s_dh, r_dh, s_dq, r_dq, s_t, r_t, s_wx, r_wx, s_wz, r_wz, s_wf, r_wf,
 ):
     z, x, c, y = (lax.axis_index(a) for a in ("z", "x", "c", "y"))
@@ -55,12 +51,12 @@
             src_ref=src, dst_ref=dst, send_sem=ss, recv_sem=rs, device_id=dev, device_id_type=MESH
         )
 
-    def c_q(j):
-        return remote(qb.at[0], qb.at[j], s_q.at[j], r_q.at[j], xdev[j])
-
-    def c_qh(i):
+    def c_q(j, p):
+        return remote(qb.at[0, p], qb.at[j, p], s_q.at[j, p], r_q.at[j, p], xdev[j])
+
+    def c_qh(i, p):
         rows = pl.ds(64 * i, 64)
-        return remote(qb.at[1 + i, rows], qb.at[3, rows], s_q.at[3 + i], r_q.at[3 + i], xdev[2 - i])
+        return remote(qb.at[1 + i, p, rows], qb.at[3, p, rows], s_q.at[3 + i, p], r_q.at[3 + i, p], xdev[2 - i])
 
     def c_st(j):
         return remote(st.at[0], st.at[j], s_st.at[j], r_st.at[j], xdev[j])
@@ -110,43 +106,68 @@
 
     c_wf = remote(wf, wfr, s_wf, r_wf, sib)
 
-    loads = [
-        pltpu.make_async_copy(qm, qb.at[0, :, 0:512], s_loc.at[0]),
-        pltpu.make_async_copy(qr, qb.at[0, :, 512:768], s_loc.at[1]),
-        pltpu.make_async_copy(og, qb.at[0, :, 768:1280], s_loc.at[2]),
-        pltpu.make_async_copy(lat, keys.at[0, 0, :, 0:512], s_loc.at[3]),
+    barrier = pltpu.get_barrier_semaphore()
+    for dev in (sib, *xdev[1:], *ydev[1:], *({"z": (z + d) % 16} for d in (1, 2, 3, 13, 14, 15))):
+        pl.semaphore_signal(barrier, inc=1, device_id=dev, device_id_type=MESH)
+    first = [
+        (krt, krv),
+        (lat, keys.at[0, 0, :, 0:512]),
+        (qm.at[:, 0:256], qb.at[0, 0, :, 0:256]),
+        (qr.at[:, 0:128], qb.at[0, 0, :, 256:384]),
+        (og.at[:, 0:256], qb.at[0, 0, :, 384:640]),
+        (qm.at[:, 256:512], qb.at[0, 1, :, 0:256]),
+        (qr.at[:, 128:256], qb.at[0, 1, :, 256:384]),
+        (og.at[:, 256:512], qb.at[0, 1, :, 384:640]),
+        (kwh, kw),
+        (vwh, vw),
+        (hoh, ho),
+        (lsh, ls),
     ]
+    loads = [pltpu.make_async_copy(a, b, s_loc.at[i]) for i, (a, b) in enumerate(first)]
     for copy in loads:
         copy.start()
-    barrier = pltpu.get_barrier_semaphore()
-    for dev in (sib, *xdev[1:], *ydev[1:]):
-        pl.semaphore_signal(barrier, inc=1, device_id=dev, device_id_type=MESH)
-
-    def greet(d, carry):
-        pl.semaphore_signal(barrier, inc=1, device_id={"z": (z + d) % 16}, device_id_type=MESH)
-        return carry
-
-    lax.fori_loop(1, 16, greet, 0)
-    keys[0, 0, :, 512:WIDE] = jnp.concatenate([krt[...].T, jnp.zeros((128, 64), BF16)], axis=1)
-    for copy in loads:
+    loads[0].wait()
+    keys[0, 0, :, 512:WIDE] = jnp.concatenate([krv[...].T, jnp.zeros((128, 64), BF16)], axis=1)
+    for copy in loads[1:8]:
         copy.wait()
-    pl.semaphore_wait(barrier, 22)
+    pl.semaphore_wait(barrier, 13)
+
+    def relay(i):
+        for d in (3, 13):
+            pl.semaphore_signal(hop.at[i], inc=1, device_id={"z": (z + d) % 16}, device_id_type=MESH)
 
     def pass_on(s):
-        @pl.when(more > 0)
-        def _():
-            c_kz(s).start()
+        if s < 3:
+
+            @pl.when(more > 0)
+            def _():
+                c_kz(s).start()
 
         c_kd(s).start()
 
-    c_q(1).start()
-    c_q(2).start()
-    pass_on(0)
-
+    for p in (0, 1):
+        c_q(1, p).start()
+        c_q(2, p).start()
+        if p == 0:
+            pass_on(0)
+    relay(0)
+
+    def rows_of(slot):
+        if slot in (0, 3):
+            return [(slot, h) for h in range(4)]
+        return [(j, 2 * (slot - 1) + h) for j in (1, 2) for h in (0, 1)]
+
+    def place_of(j, h):
+        if j in (0, 3):
+            return j, h
+        return 1 + h // 2, 2 * (j - 1) + h % 2
+
+    for copy in loads[8:]:
+        copy.wait()
     ones = jnp.ones((8, 128), F32)
     for h in range(4):
         cols = pl.ds(h * 128, 128)
-        prod = ho[:, cols].astype(F32) * qb[0, :, 768 + h * 128 : 896 + h * 128].astype(F32)
+        prod = ho[:, cols].astype(F32) * qb[0, h // 2, :, 384 + h % 2 * 128 : 512 + h % 2 * 128].astype(F32)
         sums = lax.dot_general(
             ones, prod, NT, precision=lax.Precision.HIGHEST, preferred_element_type=F32
         )
@@ -155,14 +176,16 @@
     for j in (1, 2, 3):
         c_st(j).start()
 
-    def project(j):
-        for h in range(4):
+    def project(slot):
+        for b, (j, h) in enumerate(rows_of(slot)):
+            p, k = h // 2, h % 2
             cols = pl.ds(h * 128, 128)
-            rows = pl.ds(h * 128, 128)
-            qc[j, rows, 0:512] = dot(qb[j, :, h * 128 : h * 128 + 128], kw[:, cols], NT).astype(BF16)
-            gr[j, rows, :] = dot(qb[j, :, 768 + h * 128 : 896 + h * 128], vw[:, cols], NT).astype(BF16)
-            rot = qb[j, :, 512 + h * 64 : 576 + h * 64]
-            qc[j, rows, 512:WIDE] = jnp.concatenate([rot, jnp.zeros((128, 64), BF16)], axis=1)
+            rows = pl.ds(b * 128, 128)
+            qc[slot, rows, 0:512] = dot(qb[j, p, :, k * 128 : k * 128 + 128], kw[:, cols], NT).astype(BF16)
+            gr[slot, rows, :] = dot(qb[j, p, :, 384 + k * 128 : 512 + k * 128], vw[:, cols], NT).astype(BF16)
+            rot = qb[j, p, :, 256 + k * 64 : 320 + k * 64]
+            qc[slot, rows, 512:WIDE] = jnp.concatenate([rot, jnp.zeros((128, 64), BF16)], axis=1)
+            sts[slot, 0:2, rows] = st[j, 0:2, cols]
 
     project(0)
     mix[...] = jnp.zeros_like(mix)
@@ -170,17 +193,19 @@
 
     def tile(s, j):
         kt = keys[s].reshape(256, WIDE)
-        turn = jnp.where(j == 0, x, jnp.where(j == 1, x1, jnp.where(j == 2, x3, x2)))
+        turn_a = jnp.where(j == 0, x, jnp.where(j == 3, x2, x1))
+        turn_b = jnp.where(j == 0, x, jnp.where(j == 3, x2, x3))
         far = jnp.where(s > 0, 1 << 20, 0)
         first = (2 * x + c) * 128 - far
         second = (2 * x + 1 - c) * 128 - 128 - far
         k_row = lax.broadcasted_iota(jnp.int32, (256, 1), 0)
         k_place = jnp.where(k_row < 128, k_row + first, k_row + second)
-        q_place = lax.broadcasted_iota(jnp.int32, (1, 512), 1) % 128 + (2 * turn + c) * 128
+        q_col = lax.broadcasted_iota(jnp.int32, (1, 512), 1)
+        q_place = q_col % 128 + jnp.where(q_col < 256, 2 * turn_a + c, 2 * turn_b + c) * 128
         scores = dot(kt, qc[j], NT)
-        weights = jnp.where(k_place <= q_place, jnp.exp(factor * scores - st[j, 0:1, :]), 0.0)
+        weights = jnp.where(k_place <= q_place, jnp.exp(factor * scores - sts[j, 0:1, :]), 0.0)
         slopes = dot(kt[:, 0:512], gr[j], NT)
-        dscores = weights * (slopes - st[j, 1:2, :])
+        dscores = weights * (slopes - sts[j, 1:2, :])
         w_low = weights.astype(BF16)
         d_low = dscores.astype(BF16)
         mix[j] += dot(kt, d_low, TN)
@@ -211,109 +236,121 @@
             c_y2(s, g).wait_recv()
             zs[s, 16 * g : 16 * g + 16, :] = own(s, g, y) + y1r[s, g, 0] + y2r[s, g]
 
-        @pl.when(s > 0)
+        if s > 0:
+            c_z(s).start()
+
+    def have(s, act):
+        @pl.when(zp >= s)
         def _():
-            c_z(s).start()
-
-    def each(act, last=3):
-        def step(s, carry):
             act(s)
-            return carry
-
-        lax.fori_loop(0, jnp.minimum(zp, last) + 1, step, 0)
 
     def do_dq(j):
         for h in range(4):
             cols = pl.ds(h * 128, 128)
-            m = mix[j, 0:512, cols]
+            slot, b = place_of(j, h)
+            m = mix[slot, 0:512, b * 128 : b * 128 + 128]
             high = m.astype(BF16)
             rest = (m - high.astype(F32)).astype(BF16)
             got = dot(high, kw[:, cols], TN) + dot(rest, kw[:, cols], TN)
             dqs[j, :, cols] = factor * got
         for g in range(2):
-            a = mix[j, 512:640, g * 256 : g * 256 + 128].T
-            b = mix[j, 512:640, g * 256 + 128 : g * 256 + 256].T
-            dqs[j, :, 512 + g * 128 : 640 + g * 128] = factor * jnp.concatenate(
-                [a[:, 0:64], b[:, 0:64]], axis=1
-            )
-
-    def visit(t, carry):
-        s, j = pick(ORDER_S, t), pick(ORDER_J, t)
-
-        def arrive(k):
-            @pl.when((t == {1: 1, 2: 4, 3: 12}[k]) & (zp >= k))
+            pair = []
+            for h in (2 * g, 2 * g + 1):
+                slot, b = place_of(j, h)
+                pair.append(mix[slot, 512:640, b * 128 : b * 128 + 128].T[:, 0:64])
+            dqs[j, :, 512 + g * 128 : 640 + g * 128] = factor * jnp.concatenate(pair, axis=1)
+
+    def run(*pairs):
+        def visit(t, carry):
+            s = pick([a for a, _ in pairs], t)
+
+            @pl.when(s <= zp)
             def _():
-                c_kzr(k).wait_recv()
-                pass_on(k)
-
-        arrive(1)
-        arrive(2)
-        arrive(3)
-
-        @pl.when(((t < 2) | (t == 6) | (t == 12)) & (s <= zp))
-        def _():
-            c_kd(s).wait_recv()
-
-        @pl.when(t == 2)
-        def _():
-            c_q(1).wait_recv()
-            c_q(2).wait_recv()
-            c_qh(0).start()
-            c_qh(1).start()
-            for k in (1, 2):
-                c_st(k).wait_recv()
-                project(k)
-
-        @pl.when(t == 9)
-        def _():
-            c_qh(0).wait_recv()
-            c_qh(1).wait_recv()
-            c_st(3).wait_recv()
-            project(3)
-
-        @pl.when(t == 12)
-        def _():
-            each(lambda s: c_d(s).start(), 2)
-
-        @pl.when(t == 14)
-        def _():
-            each(do_y1, 2)
-
-        @pl.when(s <= zp)
-        def _():
-            tile(s, j)
-
-        @pl.when(t == 12)
-        def _():
-            do_dq(3)
-            c_dh(0).start()
-            c_dh(1).start()
-
-        return carry
-
-    lax.fori_loop(0, 16, visit, 0)
-
-    @pl.when(zp == 3)
-    def _():
-        c_d(3).start()
-
-    for rel in (1, 0):
-        half = c if rel == 0 else 1 - c
-        for hh in (0, 1):
-            cols = pl.ds(pl.multiple_of((2 * half + hh) * 128, 128), 128)
+                tile(s, pick([b for _, b in pairs], t))
+
+            return carry
+
+        lax.fori_loop(0, len(pairs), visit, 0)
+
+    def arrive(s):
+        c_kzr(s).wait_recv()
+        pass_on(s)
+
+    def ready(s):
+        c_kd(s).wait_recv()
+
+    def halves(p):
+        for j in (1, 2):
+            c_q(j, p).wait_recv()
+        for i in (0, 1):
+            c_qh(i, p).start()
+
+    def give(s):
+        c_d(s).start()
+
+    ready(0)
+    run((0, 0))
+    have(1, arrive)
+    have(1, ready)
+    run((1, 0))
+    halves(0)
+    for j in (1, 2):
+        c_st(j).wait_recv()
+    project(1)
+    run((0, 1), (1, 1))
+    pl.semaphore_wait(hop.at[0], 2)
+    relay(1)
+    have(2, arrive)
+    halves(1)
+    have(2, ready)
+    project(2)
+    run((2, 0), (0, 2), (1, 2), (2, 1))
+    have(3, arrive)
+    for i in (0, 1):
+        c_qh(i, 0).wait_recv()
+        c_qh(i, 1).wait_recv()
+    c_st(3).wait_recv()
+    project(3)
+    have(3, ready)
+    run((3, 0), (3, 1), (3, 2), (3, 3))
+    have(3, give)
+    run((2, 2), (2, 3))
+    have(2, give)
+    have(3, do_y1)
+    run((1, 3))
+    have(1, give)
+    have(2, do_y1)
+    run((0, 3))
+    give(0)
+
+    def do_term(rel):
+        p = c if rel == 0 else 1 - c
+        for k in (0, 1):
             got = jnp.zeros((512, 128), F32)
+            wide = pl.ds(pl.multiple_of((2 * p + k) * 128, 128), 128)
             for j in range(4):
-                m = mix[j, 0:512, cols]
+                if j in (0, 3):
+                    m = mix[j, 0:512, wide]
+                else:
+                    m = mix[1 + p, 0:512, (2 * (j - 1) + k) * 128 : (2 * (j - 1) + k + 1) * 128]
                 high = m.astype(BF16)
                 rest = (m - high.astype(F32)).astype(BF16)
-                q = qb[j, :, cols]
+                q = qb[j, p, :, k * 128 : k * 128 + 128]
                 got = got + dot(jnp.concatenate([high, rest], axis=1), jnp.concatenate([q, q], axis=0))
-            term[rel, :, :, :, hh * 128 : (hh + 1) * 128] = (factor * got).reshape(16, 4, 8, 128)
-        if rel == 1:
-            c_t.start()
-    each(do_y2, 2)
+            term[rel, :, :, :, k * 128 : (k + 1) * 128] = (factor * got).reshape(16, 4, 8, 128)
+
+    do_term(1)
+    c_t.start()
+    do_dq(3)
+    c_dh(0).start()
+    c_dh(1).start()
+    have(3, do_y2)
+    have(1, do_y1)
+    do_term(0)
+    have(2, do_y2)
+    do_y1(0)
     c_t.wait_recv()
-    for j in range(4):
+    for j in (1, 2, 3, 0):
         turn = (x, x1, x3, x2)[j]
         got = (term[0, :, turn] + termr[:, turn]).reshape(128, 256)
         if j == 0:
@@ -321,21 +358,22 @@
         else:
             wxs[j] = got.astype(BF16)
             c_wx(j).start()
-
+    have(3, do_z)
+    have(1, do_y2)
     do_dq(1)
+    do_dq(2)
+    have(2, do_z)
+    do_y2(0)
+
     c_dh(1).wait_recv()
     dqs[1, 64:128, :] += dqh[1]
     c_dq(1).start()
-    do_dq(2)
     c_dh(0).wait_recv()
     dqs[2, 0:64, :] += dqh[0]
     c_dq(2).start()
-
-    @pl.when(zp == 3)
-    def _():
-        do_y1(3)
-
-    each(do_z, 2)
+    have(1, do_z)
+
+    pl.semaphore_wait(hop.at[1], 2)
     got = wx0[...]
     for j in (1, 2, 3):
         c_wx(j).wait_recv()
@@ -347,16 +385,8 @@
         return carry
 
     lax.fori_loop(1, 16, go, 0)
-
-    @pl.when(zp == 3)
-    def _():
-        do_y2(3)
-
+    do_z(0)
     do_dq(0)
-
-    @pl.when(zp == 3)
-    def _():
-        do_z(3)
 
     def wait_z(d, carry):
         c_zr(d).wait_recv()
@@ -368,24 +398,33 @@
     for j in (1, 2, 3):
         c_f(j).start()
 
+    c_dq(1).wait_recv()
+    c_dq(2).wait_recv()
+    dqs[0] += dqr[0] + dqr[1]
+    outs = [
+        pltpu.make_async_copy(dqs.at[0, :, 0:512], o_main, s_out.at[0]),
+        pltpu.make_async_copy(dqs.at[0, :, 512:768], o_rot, s_out.at[1]),
+    ]
+    for copy in outs:
+        copy.start()
+
     def wait_wz(d, total):
         c_wz(d).wait_recv()
         return total + wzr[d]
 
     wf[...] = lax.fori_loop(1, 16, wait_wz, wz[z])
     c_wf.start()
-
-    c_dq(1).wait_recv()
-    c_dq(2).wait_recv()
-    o_main[...] = dqs[0, :, 0:512] + dqr[0, :, 0:512] + dqr[1, :, 0:512]
-    o_rot[...] = dqs[0, :, 512:768] + dqr[0, :, 512:768] + dqr[1, :, 512:768]
-
     for j in range(4):
         if j > 0:
             c_f(j).wait_recv()
         rows = pl.ds(pl.multiple_of((y, y1, y3, y2)[j] * 32, 32), 32)
-        o_lat[rows, :] = fin[j, :, 0:512]
-        o_krot[rows, :] = fin[j, :, 512:640]
+        late = [
+            pltpu.make_async_copy(fin.at[j, :, 0:512], o_lat.at[rows], s_out.at[2 + 2 * j]),
+            pltpu.make_async_copy(fin.at[j, :, 512:640], o_krot.at[rows], s_out.at[3 + 2 * j]),
+        ]
+        for copy in late:
+            copy.start()
+        outs += late
     c_wf.wait_recv()
 
     @pl.when(c == 0)
@@ -398,27 +437,32 @@
         o_weight[:, 0:256] = wfr[4:8, :]
         o_weight[:, 256:512] = wf[4:8, :]
 
+    for copy in outs:
+        copy.wait()
+
     def drain(s):
-        @pl.when(more > 0)
-        def _():
-            c_kz(s).wait_send()
+        if s < 3:
+
+            @pl.when(more > 0)
+            def _():
+                c_kz(s).wait_send()
 
         c_kd(s).wait_send()
         c_d(s).wait_send()
         for g in (0, 1):
             c_y1(s, g).wait_send()
             c_y2(s, g).wait_send()
-
-        @pl.when(s > 0)
-        def _():
+        if s > 0:
             c_z(s).wait_send()
 
-    each(drain)
+    for s in range(4):
+        have(s, drain)
     c_t.wait_send()
     c_wf.wait_send()
     for i in (0, 1):
-        c_q(1 + i).wait_send()
-        c_qh(i).wait_send()
+        for p in (0, 1):
+            c_q(1 + i, p).wait_send()
+            c_qh(i, p).wait_send()
         c_dh(i).wait_send()
         c_dq(1 + i).wait_send()
     for j in (1, 2, 3):
@@ -446,7 +490,13 @@
     hbm = pl.BlockSpec(memory_space=pl.ANY)
     dma = pltpu.SemaphoreType.DMA
     scratch = [
-        pltpu.VMEM((4, 128, 1280), BF16),
+        pltpu.VMEM((512, 512), BF16),
+        pltpu.VMEM((512, 512), BF16),
+        pltpu.VMEM((128, 512), BF16),
+        pltpu.VMEM((4, 128), F32),
+        pltpu.VMEM((64, 128), BF16),
+        pltpu.VMEM((4, 2, 128, 640), BF16),
+        pltpu.VMEM((4, 8, 512), F32),
         pltpu.VMEM((4, 8, 512), F32),
         pltpu.VMEM((4, 512, WIDE), BF16),
         pltpu.VMEM((4, 512, 512), BF16),
@@ -473,8 +523,10 @@
         pltpu.VMEM((16, 8, 256), F32),
         pltpu.VMEM((8, 256), F32),
         pltpu.VMEM((8, 256), F32),
-        dma((4,)),
-        dma((5,)), dma((5,)),
+        dma((12,)),
+        dma((10,)),
+        pltpu.SemaphoreType.REGULAR((2,)),
+        dma((5, 2)), dma((5, 2)),
         dma((4,)), dma((4,)),
         dma((4,)), dma((5,)),
         dma((4,)), dma((4,)),
@@ -499,8 +551,8 @@
             jax.ShapeDtypeStruct((128, 128), F32),
             jax.ShapeDtypeStruct((4, 512), F32),
         ),
-        in_specs=[hbm, hbm, hbm, v, v, v, v, hbm, v],
-        out_specs=(v,) * 5,
+        in_specs=[hbm] * 9,
+        out_specs=(hbm,) * 4 + (v,),
         scratch_shapes=scratch,
         compiler_params=pltpu.CompilerParams(
             collective_id=0, has_side_effects=True, vmem_limit_bytes=56 * 1024 * 1024

time: 76.3 us -> 69.4 us (0.910)
  the two profiles are of different devices: /device:TPU:97 before, /device:TPU:1 now
where the time goes in v3:
time: 69.4 us; the launch traced here: 69.2 us
  Pallas kernels  68.6 us (99%)
    pallas_call x1, Pallas kernels, per_device(): pl.pallas_call(body, out_shape=(jax.ShapeDtypeStruct((128, 512), F32), ja...  66.6 us
    pallas_call x1, Pallas kernels, per_device(): pl.pallas_call(put_out, out_shape=(jax.ShapeDtypeStruct((128, 512), F32),...  1.98 us

profile of v3, /device:TPU:1, one launch (start us, length us, event | category | flops | bytes accessed | tf_op | source)
XLA Modules:
  0.0 69.2 jit_solution(17430863066013509205)
XLA Ops:
  0.6 66.6 %shard_map.128 = (f32[128,512]{1,0:T(8,128)}, f32[128,256]{1,0:T(8,128)}, f32[128,512]{1,0:T(8,128)}, f32[128,128]{1,0:T(8,128)}, f32[4,512]{1,0:T(4,128)}) custom-call(bf16[128,512]{1,0:T(8,128)(2,1)} %qm.1, bf16[128,256]{1,0:T(8,128)(2,1)} %qr.1, bf16[128,512]{1,0:T(8,128)(2,1)} %lat.1, bf16[64,128]{1,0:T(8,128)(2,1)} %bitcast.2, bf16[512,512]{1,0:T(8,128)(2,1)} %kwh.1, ...), custom_call_target="tpu_custom_call" | custom-call | tf_op jit(solution)/shard_map/pallas_call | solution.py:545
  67.2 2.0 %shard_map.129 = (f32[128,512]{1,0:T(8,128)}, f32[128,256]{1,0:T(8,128)}, f32[128,512]{1,0:T(8,128)}, f32[64,128]{1,0:T(8,128)}, f32[4,512]{1,0:T(4,128)}) custom-call(f32[128,512]{1,0:T(8,128)} %get-tuple-element.15.a, f32[128,256]{1,0:T(8,128)} %get-tuple-element.16.b, f32[128,512]{1,0:T(8,128)} %get-tuple-element.17.d, f32[128,128]{1,0:T(8,128)} %get-tuple-element.18.e, ...), custom_call_target="tpu_custom_call" | custom-call | tf_op jit(solution)/shard_map/pallas_call | solution.py:561

commit v4 on v3

--- a/solution.py
+++ b/solution.py
@@ -11,6 +11,7 @@
 F32 = jnp.float32
 BF16 = jnp.bfloat16
 WIDE = 640
+LOG2E = 1.4426950408889634
 NT = (((1,), (1,)), ((), ()))
 TN = (((0,), (0,)), ((), ()))
 
@@ -30,9 +31,9 @@
 def body(
     qm, qr, lat, krt, kwh, vwh, hoh, og, lsh,
     o_main, o_rot, o_lat, o_krot, o_weight,
-    kw, vw, ho, ls, krv, qb, st, sts, qc, gr, keys, mix, part, dsum, y1s, y1r, y2s, y2r, zs, zr, fin,
+    krots, kw, vw, ho, ls, krv, qb, st, sts, qc, gr, keys, mix, part, dsum, y1s, y1r, y2s, y2r, zs, zr, fin,
     dqs, dqh, dqr, term, termr, wx0, wxs, wxr, wz, wzr, wf, wfr,
-    s_loc, s_out, hop, s_q, r_q, s_st, r_st, s_kz, r_kz, s_kd, r_kd, s_d, r_d, s_y1, r_y1, s_y2, r_y2,
+    s_loc, hop, s_q, r_q, s_st, r_st, s_kz, r_kz, s_kd, r_kd, s_d, r_d, s_y1, r_y1, s_y2, r_y2,
     s_z, r_z, s_f, r_f, s_dh, r_dh, s_dq, r_dq, s_t, r_t, s_wx, r_wx, s_wz, r_wz, s_wf, r_wf,
 ):
     z, x, c, y = (lax.axis_index(a) for a in ("z", "x", "c", "y"))
@@ -59,6 +60,8 @@
         return remote(qb.at[1 + i, p, rows], qb.at[3, p, rows], s_q.at[3 + i, p], r_q.at[3 + i, p], xdev[2 - i])
 
     def c_st(j):
+        if j == 3:
+            return remote(st.at[1], st.at[3], s_st.at[3], r_st.at[3], xdev[2])
         return remote(st.at[0], st.at[j], s_st.at[j], r_st.at[j], xdev[j])
 
     def c_kz(s):
@@ -107,7 +110,7 @@
     c_wf = remote(wf, wfr, s_wf, r_wf, sib)
 
     barrier = pltpu.get_barrier_semaphore()
-    for dev in (sib, *xdev[1:], *ydev[1:], *({"z": (z + d) % 16} for d in (1, 2, 3, 13, 14, 15))):
+    for dev in (sib, *xdev[1:3], *ydev[1:3], {"z": (z + 1) % 16}, {"z": (z + 15) % 16}):
         pl.semaphore_signal(barrier, inc=1, device_id=dev, device_id_type=MESH)
     first = [
         (krt, krv),
@@ -130,11 +133,14 @@
     keys[0, 0, :, 512:WIDE] = jnp.concatenate([krv[...].T, jnp.zeros((128, 64), BF16)], axis=1)
     for copy in loads[1:8]:
         copy.wait()
-    pl.semaphore_wait(barrier, 13)
+    pl.semaphore_wait(barrier, 7)
 
     def relay(i):
-        for d in (3, 13):
+        for d in (1 << i, 16 - (1 << i)):
             pl.semaphore_signal(hop.at[i], inc=1, device_id={"z": (z + d) % 16}, device_id_type=MESH)
+        if i == 0:
+            for dev in (*xdev[1:3], *ydev[1:3]):
+                pl.semaphore_signal(hop.at[i], inc=1, device_id=dev, device_id_type=MESH)
 
     def pass_on(s):
         if s < 3:
@@ -145,11 +151,9 @@
 
         c_kd(s).start()
 
-    for p in (0, 1):
-        c_q(1, p).start()
-        c_q(2, p).start()
-        if p == 0:
-            pass_on(0)
+    c_q(1, 0).start()
+    c_q(2, 0).start()
+    pass_on(0)
     relay(0)
 
     def rows_of(slot):
@@ -172,8 +176,8 @@
             ones, prod, NT, precision=lax.Precision.HIGHEST, preferred_element_type=F32
         )
         st[0, 1:2, cols] = sums[0:1, :]
-        st[0, 0:1, cols] = ls[h : h + 1, :]
-    for j in (1, 2, 3):
+        st[0, 0:1, cols] = LOG2E * ls[h : h + 1, :]
+    for j in (1, 2):
         c_st(j).start()
 
     def project(slot):
@@ -203,7 +207,9 @@
         q_col = lax.broadcasted_iota(jnp.int32, (1, 512), 1)
         q_place = q_col % 128 + jnp.where(q_col < 256, 2 * turn_a + c, 2 * turn_b + c) * 128
         scores = dot(kt, qc[j], NT)
-        weights = jnp.where(k_place <= q_place, jnp.exp(factor * scores - sts[j, 0:1, :]), 0.0)
+        weights = jnp.where(
+            k_place <= q_place, jnp.exp2((factor * LOG2E) * scores - sts[j, 0:1, :]), 0.0
+        )
         slopes = dot(kt[:, 0:512], gr[j], NT)
         dscores = weights * (slopes - sts[j, 1:2, :])
         w_low = weights.astype(BF16)
@@ -221,20 +227,20 @@
     def do_y1(s):
         c_d(s).wait_recv()
         for g in (0, 1):
-            y1s[s, g, 0] = own(s, g, (y1, y3)[g])
-            y1s[s, g, 1] = own(s, g, y2)
+            y1s[s, g, 0] = own(s, g, (y1, y3)[g]).astype(BF16)
+            y1s[s, g, 1] = own(s, g, y2).astype(BF16)
             c_y1(s, g).start()
 
     def do_y2(s):
         for g in (0, 1):
             c_y1(s, g).wait_recv()
-            y2s[s, g] = own(s, g, (y3, y1)[g]) + y1r[s, g, 1]
+            y2s[s, g] = own(s, g, (y3, y1)[g]) + y1r[s, g, 1].astype(F32)
             c_y2(s, g).start()
 
     def do_z(s):
         for g in (0, 1):
             c_y2(s, g).wait_recv()
-            zs[s, 16 * g : 16 * g + 16, :] = own(s, g, y) + y1r[s, g, 0] + y2r[s, g]
+            zs[s, 16 * g : 16 * g + 16, :] = own(s, g, y) + y1r[s, g, 0].astype(F32) + y2r[s, g]
 
         if s > 0:
             c_z(s).start()
@@ -290,45 +296,58 @@
 
     ready(0)
     run((0, 0))
+    pl.semaphore_wait(hop.at[0], 6)
+    relay(1)
     have(1, arrive)
+    c_q(1, 1).start()
+    c_q(2, 1).start()
     have(1, ready)
     run((1, 0))
     halves(0)
     for j in (1, 2):
         c_st(j).wait_recv()
+    c_st(3).start()
     project(1)
     run((0, 1), (1, 1))
-    pl.semaphore_wait(hop.at[0], 2)
-    relay(1)
+    pl.semaphore_wait(hop.at[1], 2)
+    relay(2)
+    halves(1)
+    project(2)
+    run((0, 2))
     have(2, arrive)
-    halves(1)
+    run((1, 2))
     have(2, ready)
-    project(2)
-    run((2, 0), (0, 2), (1, 2), (2, 1))
-    have(3, arrive)
+    run((2, 0), (2, 1), (2, 2))
     for i in (0, 1):
         c_qh(i, 0).wait_recv()
         c_qh(i, 1).wait_recv()
     c_st(3).wait_recv()
     project(3)
-    have(3, ready)
-    run((3, 0), (3, 1), (3, 2), (3, 3))
-    have(3, give)
-    run((2, 2), (2, 3))
+    have(3, arrive)
+    run((2, 3))
     have(2, give)
-    have(3, do_y1)
     run((1, 3))
     have(1, give)
-    have(2, do_y1)
     run((0, 3))
     give(0)
-
-    def do_term(rel):
+    have(2, do_y1)
+    have(3, ready)
+    run((3, 3))
+    do_dq(3)
+    c_dh(0).start()
+    c_dh(1).start()
+    have(1, do_y1)
+    run((3, 1))
+    do_y1(0)
+    run((3, 2))
+    have(2, do_y2)
+
+    def do_term(rel, slots):
         p = c if rel == 0 else 1 - c
         for k in (0, 1):
             got = jnp.zeros((512, 128), F32)
             wide = pl.ds(pl.multiple_of((2 * p + k) * 128, 128), 128)
-            for j in range(4):
+            for j in slots:
                 if j in (0, 3):
                     m = mix[j, 0:512, wide]
                 else:
@@ -337,20 +356,23 @@
                 rest = (m - high.astype(F32)).astype(BF16)
                 q = qb[j, p, :, k * 128 : k * 128 + 128]
                 got = got + dot(jnp.concatenate([high, rest], axis=1), jnp.concatenate([q, q], axis=0))
-            term[rel, :, :, :, k * 128 : (k + 1) * 128] = (factor * got).reshape(16, 4, 8, 128)
-
-    do_term(1)
+            got = (factor * got).reshape(16, 4, 8, 128)
+            if len(slots) == 1:
+                got = got + term[rel, :, :, :, k * 128 : (k + 1) * 128]
+            term[rel, :, :, :, k * 128 : (k + 1) * 128] = got
+
+    do_term(1, (1, 2, 3))
+    do_term(0, (1, 2, 3))
+    run((3, 0))
+    have(3, give)
+    do_term(1, (0,))
     c_t.start()
-    do_dq(3)
-    c_dh(0).start()
-    c_dh(1).start()
-    have(3, do_y2)
-    have(1, do_y1)
-    do_term(0)
-    have(2, do_y2)
-    do_y1(0)
+    do_term(0, (0,))
+    have(1, do_y2)
+    have(3, do_y1)
+    do_y2(0)
     c_t.wait_recv()
-    for j in (1, 2, 3, 0):
+    for j in (3, 1, 2, 0):
         turn = (x, x1, x3, x2)[j]
         got = (term[0, :, turn] + termr[:, turn]).reshape(128, 256)
         if j == 0:
@@ -358,22 +380,22 @@
         else:
             wxs[j] = got.astype(BF16)
             c_wx(j).start()
-    have(3, do_z)
-    have(1, do_y2)
+    have(2, do_z)
+
     do_dq(1)
-    do_dq(2)
-    have(2, do_z)
-    do_y2(0)
-
     c_dh(1).wait_recv()
     dqs[1, 64:128, :] += dqh[1]
     c_dq(1).start()
+    do_dq(2)
     c_dh(0).wait_recv()
     dqs[2, 0:64, :] += dqh[0]
     c_dq(2).start()
+    have(3, do_y2)
     have(1, do_z)
-
-    pl.semaphore_wait(hop.at[1], 2)
+    do_z(0)
+    do_dq(0)
+
+    pl.semaphore_wait(hop.at[2], 2)
     got = wx0[...]
     for j in (1, 2, 3):
         c_wx(j).wait_recv()
@@ -385,8 +407,7 @@
         return carry
 
     lax.fori_loop(1, 16, go, 0)
-    do_z(0)
-    do_dq(0)
+    have(3, do_z)
 
     def wait_z(d, carry):
         c_zr(d).wait_recv()
@@ -394,19 +415,14 @@
         return carry
 
     lax.fori_loop(1, more + 1, wait_z, 0)
-    fin[0] = zs[0]
+    fin[0] = zs[0].astype(BF16)
     for j in (1, 2, 3):
         c_f(j).start()
 
     c_dq(1).wait_recv()
     c_dq(2).wait_recv()
-    dqs[0] += dqr[0] + dqr[1]
-    outs = [
-        pltpu.make_async_copy(dqs.at[0, :, 0:512], o_main, s_out.at[0]),
-        pltpu.make_async_copy(dqs.at[0, :, 512:768], o_rot, s_out.at[1]),
-    ]
-    for copy in outs:
-        copy.start()
+    o_main[...] = dqs[0, :, 0:512] + dqr[0, :, 0:512] + dqr[1, :, 0:512]
+    o_rot[...] = dqs[0, :, 512:768] + dqr[0, :, 512:768] + dqr[1, :, 512:768]
 
     def wait_wz(d, total):
         c_wz(d).wait_recv()
@@ -418,13 +434,10 @@
         if j > 0:
             c_f(j).wait_recv()
         rows = pl.ds(pl.multiple_of((y, y1, y3, y2)[j] * 32, 32), 32)
-        late = [
-            pltpu.make_async_copy(fin.at[j, :, 0:512], o_lat.at[rows], s_out.at[2 + 2 * j]),
-            pltpu.make_async_copy(fin.at[j, :, 512:640], o_krot.at[rows], s_out.at[3 + 2 * j]),
-        ]
-        for copy in late:
-            copy.start()
-        outs += late
+        got = zs[0] if j == 0 else fin[j].astype(F32)
+        o_lat[rows, :] = got[:, 0:512]
+        krots[rows, :] = got[:, 512:640]
+    o_krot[...] = krots[...].T[0:64, :]
     c_wf.wait_recv()
 
     @pl.when(c == 0)
@@ -436,9 +449,6 @@
     def _():
         o_weight[:, 0:256] = wfr[4:8, :]
         o_weight[:, 256:512] = wf[4:8, :]
-
-    for copy in outs:
-        copy.wait()
 
     def drain(s):
         if s < 3:
@@ -477,12 +487,13 @@
     lax.fori_loop(1, 16, drain_wz, 0)
 
 
-def put_out(a, b, d, e, f, oa, ob, od, oe, of):
-    oa[...] = a[...]
-    ob[...] = b[...]
-    od[...] = d[...]
-    oe[...] = e[...].T[0:64, :]
-    of[...] = f[...]
+def put_out(*refs):
+    ends, sems = refs[5:10], refs[10]
+    copies = [pltpu.make_async_copy(a, b, sems.at[i]) for i, (a, b) in enumerate(zip(refs[:5], ends))]
+    for copy in copies:
+        copy.start()
+    for copy in copies:
+        copy.wait()
 
 
 def per_device(query_main, query_rotary, latent, key_rotary, key_weight, value_weight, head_output, output_grad, row_logsum):
@@ -490,6 +501,7 @@
     hbm = pl.BlockSpec(memory_space=pl.ANY)
     dma = pltpu.SemaphoreType.DMA
     scratch = [
+        pltpu.VMEM((128, 128), F32),
         pltpu.VMEM((512, 512), BF16),
         pltpu.VMEM((512, 512), BF16),
         pltpu.VMEM((128, 512), BF16),
@@ -504,13 +516,13 @@
         pltpu.VMEM((4, WIDE, 512), F32),
         pltpu.VMEM((4, 2, 128, WIDE), F32),
         pltpu.VMEM((4, 128, WIDE), F32),
-        pltpu.VMEM((4, 2, 2, 16, WIDE), F32),
-        pltpu.VMEM((4, 2, 2, 16, WIDE), F32),
+        pltpu.VMEM((4, 2, 2, 16, WIDE), BF16),
+        pltpu.VMEM((4, 2, 2, 16, WIDE), BF16),
         pltpu.VMEM((4, 2, 16, WIDE), F32),
         pltpu.VMEM((4, 2, 16, WIDE), F32),
         pltpu.VMEM((4, 32, WIDE), F32),
         pltpu.VMEM((4, 32, WIDE), F32),
-        pltpu.VMEM((4, 32, WIDE), F32),
+        pltpu.VMEM((4, 32, WIDE), BF16),
         pltpu.VMEM((4, 128, 768), F32),
         pltpu.VMEM((2, 64, 768), F32),
         pltpu.VMEM((2, 128, 768), F32),
@@ -524,8 +536,7 @@
         pltpu.VMEM((8, 256), F32),
         pltpu.VMEM((8, 256), F32),
         dma((12,)),
-        dma((10,)),
-        pltpu.SemaphoreType.REGULAR((2,)),
+        pltpu.SemaphoreType.REGULAR((3,)),
         dma((5, 2)), dma((5, 2)),
         dma((4,)), dma((4,)),
         dma((4,)), dma((5,)),
@@ -545,14 +556,14 @@
     got = pl.pallas_call(
         body,
         out_shape=(
-            jax.ShapeDtypeStruct((128, 512), F32),
-            jax.ShapeDtypeStruct((128, 256), F32),
-            jax.ShapeDtypeStruct((128, 512), F32),
-            jax.ShapeDtypeStruct((128, 128), F32),
-            jax.ShapeDtypeStruct((4, 512), F32),
+            pltpu.VMEM((128, 512), F32),
+            pltpu.VMEM((128, 256), F32),
+            pltpu.VMEM((128, 512), F32),
+            pltpu.VMEM((64, 128), F32),
+            pltpu.VMEM((4, 512), F32),
         ),
         in_specs=[hbm] * 9,
-        out_specs=(hbm,) * 4 + (v,),
+        out_specs=(v,) * 5,
         scratch_shapes=scratch,
         compiler_params=pltpu.CompilerParams(
             collective_id=0, has_side_effects=True, vmem_limit_bytes=56 * 1024 * 1024
@@ -568,8 +579,9 @@
             jax.ShapeDtypeStruct((4, 512), F32),
         ),
         in_specs=[v] * 5,
-        out_specs=(v,) * 5,
-    )(*got)
+        out_specs=(hbm,) * 5,
+        scratch_shapes=[dma((5,))],
+    )(*(pltpu.with_memory_space_constraint(a, pltpu.VMEM) for a in got))
     return main, rot, lat, krot.T, weight
 
 

time: 69.4 us -> 61.4 us (0.88)
  Pallas kernels: 68.6 us -> 60.4 us
    pallas_call x1, Pallas kernels: 66.6 us -> 59.5 us  [per_device(): pl.pallas_call(body, out_shape=(pltpu.VMEM((128, 512), F32), pltpu.VMEM((...]
    pallas_call x1, Pallas kernels: 1.98 us -> 0.88 us  [per_device(): pl.pallas_call(put_out, out_shape=(jax.ShapeDtypeStruct((128, 512), F32),...]
where the time goes in v4:
time: 61.4 us; the launch traced here: 61.2 us
  Pallas kernels  60.4 us (98%)
  between operations  0.8 us (1%)
    pallas_call x1, Pallas kernels, per_device(): pl.pallas_call(body, out_shape=(pltpu.VMEM((128, 512), F32), pltpu.VMEM((...  59.5 us

profile of v4, /device:TPU:1, one launch (start us, length us, event | category | flops | bytes accessed | tf_op | source)
XLA Modules:
  0.0 61.2 jit_solution(2544234543928908210)
XLA Ops:
  0.6 59.5 %shard_map.128 = (f32[128,512]{1,0:T(8,128)S(1)}, f32[128,256]{1,0:T(8,128)S(1)}, f32[128,512]{1,0:T(8,128)S(1)}, f32[64,128]{1,0:T(8,128)S(1)}, f32[4,512]{1,0:T(4,128)S(1)}) custom-call(bf16[128,512]{1,0:T(8,128)(2,1)} %qm.1, bf16[128,256]{1,0:T(8,128)(2,1)} %qr.1, bf16[128,512]{1,0:T(8,128)(2,1)} %lat.1, bf16[64,128]{1,0:T(8,128)(2,1)} %bitcast.2, ...), custom_call_target="tpu_custom_call" | custom-call | tf_op jit(solution)/shard_map/pallas_call | solution.py:556
  60.1 0.9 %shard_map.129 = (f32[128,512]{1,0:T(8,128)}, f32[128,256]{1,0:T(8,128)}, f32[128,512]{1,0:T(8,128)}, f32[64,128]{1,0:T(8,128)}, f32[4,512]{1,0:T(4,128)}) custom-call(f32[128,512]{1,0:T(8,128)S(1)} %get-tuple-element.15.refs_0_, f32[128,256]{1,0:T(8,128)S(1)} %get-tuple-element.16.refs_1_, f32[128,512]{1,0:T(8,128)S(1)} %get-tuple-element.17.refs_2_, ...), custom_call_target="tpu_custom_call" | custom-call | tf_op jit(solution)/shard_map/pallas_call | solution.py:572

commit v5 on v4

--- a/solution.py
+++ b/solution.py
@@ -31,10 +31,10 @@
 def body(
     qm, qr, lat, krt, kwh, vwh, hoh, og, lsh,
     o_main, o_rot, o_lat, o_krot, o_weight,
-    krots, kw, vw, ho, ls, krv, qb, st, sts, qc, gr, keys, mix, part, dsum, y1s, y1r, y2s, y2r, zs, zr, fin,
-    dqs, dqh, dqr, term, termr, wx0, wxs, wxr, wz, wzr, wf, wfr,
+    krots, kv, ho, ls, krv, qb, st, sts, qc, gr, keys, mix, part, dsum, y1s, y1r, y2s, y2r, zs, zr, fin,
+    dqs, dqh, dqr, term, termr, wx0, wxs, wxr, wz, wzr,
     s_loc, hop, s_q, r_q, s_st, r_st, s_kz, r_kz, s_kd, r_kd, s_d, r_d, s_y1, r_y1, s_y2, r_y2,
-    s_z, r_z, s_f, r_f, s_dh, r_dh, s_dq, r_dq, s_t, r_t, s_wx, r_wx, s_wz, r_wz, s_wf, r_wf,
+    s_z, r_z, s_f, r_f, s_dh, r_dh, s_dq, r_dq, s_t, r_t, s_wx, r_wx, s_wz, r_wz,
 ):
     z, x, c, y = (lax.axis_index(a) for a in ("z", "x", "c", "y"))
     factor = 192.0 ** (-0.5)
@@ -53,22 +53,22 @@
         )
 
     def c_q(j, p):
-        return remote(qb.at[0, p], qb.at[j, p], s_q.at[j, p], r_q.at[j, p], xdev[j])
+        return remote(qb.at[0, p], qb.at[j, p], s_q.at[0], r_q.at[p], xdev[j])
 
     def c_qh(i, p):
         rows = pl.ds(64 * i, 64)
-        return remote(qb.at[1 + i, p, rows], qb.at[3, p, rows], s_q.at[3 + i, p], r_q.at[3 + i, p], xdev[2 - i])
+        return remote(qb.at[1 + i, p, rows], qb.at[3, p, rows], s_q.at[1], r_q.at[2], xdev[2 - i])
 
     def c_st(j):
         if j == 3:
-            return remote(st.at[1], st.at[3], s_st.at[3], r_st.at[3], xdev[2])
-        return remote(st.at[0], st.at[j], s_st.at[j], r_st.at[j], xdev[j])
+            return remote(st.at[1], st.at[3], s_st.at[1], r_st.at[1], xdev[2])
+        return remote(st.at[0], st.at[j], s_st.at[0], r_st.at[0], xdev[j])
 
     def c_kz(s):
-        return remote(keys.at[s, 0], keys.at[s + 1, 0], s_kz.at[s], r_kz.at[s + 1], {"z": z + 1})
+        return remote(keys.at[s, 0], keys.at[s + 1, 0], s_kz.at[s], r_kz.at[s], {"z": z + 1})
 
     def c_kzr(s):
-        return remote(keys.at[s, 0], keys.at[s, 0], s_kz.at[s], r_kz.at[s], {"z": z - 1})
+        return remote(keys.at[s - 1, 0], keys.at[s, 0], s_kz.at[s - 1], r_kz.at[s - 1], {"z": z - 1})
 
     def c_kd(s):
         return remote(keys.at[s, 0], keys.at[s, 1], s_kd.at[s], r_kd.at[s], sib)
@@ -77,62 +77,68 @@
         return remote(part.at[s, 1], dsum.at[s], s_d.at[s], r_d.at[s], sib)
 
     def c_y1(s, g):
-        return remote(y1s.at[s, g], y1r.at[s, g], s_y1.at[s, g], r_y1.at[s, g], ydev[1 + g])
+        return remote(y1s.at[s, g], y1r.at[s, g], s_y1.at[s], r_y1.at[s], ydev[1 + g])
 
     def c_y2(s, g):
-        return remote(y2s.at[s, g], y2r.at[s, g], s_y2.at[s, g], r_y2.at[s, g], ydev[2 - g])
+        return remote(y2s.at[s, g], y2r.at[s, g], s_y2.at[s], r_y2.at[s], ydev[2 - g])
 
     def c_z(s):
-        return remote(zs.at[s], zr.at[s], s_z.at[s], r_z.at[s], {"z": z - s})
+        return remote(zs.at[s], zr.at[s], s_z.at[s - 1], r_z.at[s - 1], {"z": z - s})
 
     def c_zr(s):
-        return remote(zs.at[s], zr.at[s], s_z.at[s], r_z.at[s], {"z": z + s})
+        return remote(zs.at[s], zr.at[s], s_z.at[s - 1], r_z.at[s - 1], {"z": z + s})
 
     def c_f(j):
-        return remote(fin.at[0], fin.at[j], s_f.at[j], r_f.at[j], ydev[j])
+        return remote(fin.at[0], fin.at[j], s_f.at[0], r_f.at[0], ydev[j])
 
     def c_dh(i):
         rows = pl.ds(64 * i, 64)
-        return remote(dqs.at[3, rows], dqh.at[i], s_dh.at[i], r_dh.at[i], xdev[1 + i])
+        return remote(dqs.at[3, rows], dqh.at[i], s_dh.at[0], r_dh.at[i], xdev[1 + i])
 
     def c_dq(j):
-        return remote(dqs.at[j], dqr.at[j - 1], s_dq.at[j], r_dq.at[j], xdev[j])
-
-    c_t = remote(term.at[1], termr, s_t, r_t, sib)
+        return remote(dqs.at[j], dqr.at[j - 1], s_dq.at[0], r_dq.at[0], xdev[j])
+
+    def c_t(j):
+        turn = (x, x1, x3, x2)[j]
+        return remote(term.at[1, :, turn], termr.at[:, turn], s_t.at[0], r_t.at[j], sib)
 
     def c_wx(j):
-        return remote(wxs.at[j], wxr.at[j], s_wx.at[j], r_wx.at[j], xdev[j])
-
-    def c_wz(d):
+        return remote(wxs.at[j], wxr.at[j], s_wx.at[0], r_wx.at[0], xdev[j])
+
+    def c_wz(k, d):
         to = (z + d) % 16
-        return remote(wz.at[to], wzr.at[d], s_wz.at[d], r_wz.at[d], {"z": to})
-
-    c_wf = remote(wf, wfr, s_wf, r_wf, sib)
+        own = c if k == 0 else 1 - c
+        dev = {"z": to, "c": own}
+        return remote(wz.at[own * 16 + to], wzr.at[16 * k + d], s_wz.at[0], r_wz.at[0], dev)
+
+    def w_all(ref, sem):
+        pltpu.make_async_copy(ref, ref, sem).wait()
 
     barrier = pltpu.get_barrier_semaphore()
     for dev in (sib, *xdev[1:3], *ydev[1:3], {"z": (z + 1) % 16}, {"z": (z + 15) % 16}):
         pl.semaphore_signal(barrier, inc=1, device_id=dev, device_id_type=MESH)
     first = [
-        (krt, krv),
-        (lat, keys.at[0, 0, :, 0:512]),
-        (qm.at[:, 0:256], qb.at[0, 0, :, 0:256]),
-        (qr.at[:, 0:128], qb.at[0, 0, :, 256:384]),
-        (og.at[:, 0:256], qb.at[0, 0, :, 384:640]),
-        (qm.at[:, 256:512], qb.at[0, 1, :, 0:256]),
-        (qr.at[:, 128:256], qb.at[0, 1, :, 256:384]),
-        (og.at[:, 256:512], qb.at[0, 1, :, 384:640]),
-        (kwh, kw),
-        (vwh, vw),
-        (hoh, ho),
-        (lsh, ls),
+        (krt, krv, 0),
+        (lat, keys.at[0, 0, :, 0:512], 1),
+        (qm.at[:, 0:256], qb.at[0, 0, :, 0:256], 2),
+        (qr.at[:, 0:128], qb.at[0, 0, :, 256:384], 2),
+        (og.at[:, 0:256], qb.at[0, 0, :, 384:640], 2),
+        (qm.at[:, 256:512], qb.at[0, 1, :, 0:256], 2),
+        (qr.at[:, 128:256], qb.at[0, 1, :, 256:384], 2),
+        (og.at[:, 256:512], qb.at[0, 1, :, 384:640], 2),
+        (kwh, kv.at[0], 3),
+        (vwh, kv.at[1], 3),
+        (hoh, ho, 4),
+        (lsh, ls, 5),
     ]
-    loads = [pltpu.make_async_copy(a, b, s_loc.at[i]) for i, (a, b) in enumerate(first)]
+    kw, vw = kv.at[0], kv.at[1]
+    loads = [pltpu.make_async_copy(a, b, s_loc.at[i]) for a, b, i in first]
     for copy in loads:
         copy.start()
     loads[0].wait()
     keys[0, 0, :, 512:WIDE] = jnp.concatenate([krv[...].T, jnp.zeros((128, 64), BF16)], axis=1)
-    for copy in loads[1:8]:
-        copy.wait()
+    loads[1].wait()
+    w_all(qb.at[0], s_loc.at[2])
     pl.semaphore_wait(barrier, 7)
 
     def relay(i):
@@ -166,7 +172,8 @@
             return j, h
         return 1 + h // 2, 2 * (j - 1) + h % 2
 
-    for copy in loads[8:]:
+    w_all(kv, s_loc.at[3])
+    for copy in loads[10:]:
         copy.wait()
     ones = jnp.ones((8, 128), F32)
     for h in range(4):
@@ -195,7 +202,7 @@
     mix[...] = jnp.zeros_like(mix)
     part[...] = jnp.zeros_like(part)
 
-    def tile(s, j):
+    def tile(s, j, masked):
         kt = keys[s].reshape(256, WIDE)
         turn_a = jnp.where(j == 0, x, jnp.where(j == 3, x2, x1))
         turn_b = jnp.where(j == 0, x, jnp.where(j == 3, x2, x3))
@@ -207,14 +214,14 @@
         q_col = lax.broadcasted_iota(jnp.int32, (1, 512), 1)
         q_place = q_col % 128 + jnp.where(q_col < 256, 2 * turn_a + c, 2 * turn_b + c) * 128
         scores = dot(kt, qc[j], NT)
-        weights = jnp.where(
-            k_place <= q_place, jnp.exp2((factor * LOG2E) * scores - sts[j, 0:1, :]), 0.0
-        )
+        weights = jnp.exp2((factor * LOG2E) * scores - sts[j, 0:1, :])
+        if masked:
+            weights = jnp.where(k_place <= q_place, weights, 0.0)
         slopes = dot(kt[:, 0:512], gr[j], NT)
         dscores = weights * (slopes - sts[j, 1:2, :])
         w_low = weights.astype(BF16)
         d_low = dscores.astype(BF16)
-        mix[j] += dot(kt, d_low, TN)
+        mix[j, 0:576, :] += dot(kt[:, 0:576], d_low, TN)
         main = factor * dot(d_low, qc[j, :, 0:512]) + dot(w_low, gr[j])
         rest = factor * dot(d_low, qc[j, :, 512:WIDE])
         part[s, :, :, 0:512] += main.reshape(2, 128, 512)
@@ -232,16 +239,15 @@
             c_y1(s, g).start()
 
     def do_y2(s):
+        w_all(y1r.at[s], r_y1.at[s])
         for g in (0, 1):
-            c_y1(s, g).wait_recv()
             y2s[s, g] = own(s, g, (y3, y1)[g]) + y1r[s, g, 1].astype(F32)
             c_y2(s, g).start()
 
     def do_z(s):
+        w_all(y2r.at[s], r_y2.at[s])
         for g in (0, 1):
-            c_y2(s, g).wait_recv()
             zs[s, 16 * g : 16 * g + 16, :] = own(s, g, y) + y1r[s, g, 0].astype(F32) + y2r[s, g]
-
         if s > 0:
             c_z(s).start()
 
@@ -272,7 +278,7 @@
 
             @pl.when(s <= zp)
             def _():
-                tile(s, pick([b for _, b in pairs], t))
+                tile(s, pick([b for _, b in pairs], t), any(a == 0 for a, _ in pairs))
 
             return carry
 
@@ -286,8 +292,7 @@
         c_kd(s).wait_recv()
 
     def halves(p):
-        for j in (1, 2):
-            c_q(j, p).wait_recv()
+        w_all(qb.at[1:3, p], r_q.at[p])
         for i in (0, 1):
             c_qh(i, p).start()
 
@@ -304,8 +309,7 @@
     have(1, ready)
     run((1, 0))
     halves(0)
-    for j in (1, 2):
-        c_st(j).wait_recv()
+    w_all(st.at[1:3], r_st.at[0])
     c_st(3).start()
     project(1)
     run((0, 1), (1, 1))
@@ -318,9 +322,9 @@
     run((1, 2))
     have(2, ready)
     run((2, 0), (2, 1), (2, 2))
-    for i in (0, 1):
-        c_qh(i, 0).wait_recv()
-        c_qh(i, 1).wait_recv()
+    pl.semaphore_wait(hop.at[2], 2)
+    pl.semaphore_signal(hop.at[3], inc=1, device_id=sib, device_id_type=MESH)
+    w_all(qb.at[3], r_q.at[2])
     c_st(3).wait_recv()
     project(3)
     have(3, arrive)
@@ -357,7 +361,7 @@
                 q = qb[j, p, :, k * 128 : k * 128 + 128]
                 got = got + dot(jnp.concatenate([high, rest], axis=1), jnp.concatenate([q, q], axis=0))
             got = (factor * got).reshape(16, 4, 8, 128)
-            if len(slots) == 1:
+            if slots == (0,):
                 got = got + term[rel, :, :, :, k * 128 : (k + 1) * 128]
             term[rel, :, :, :, k * 128 : (k + 1) * 128] = got
 
@@ -366,48 +370,51 @@
     run((3, 0))
     have(3, give)
     do_term(1, (0,))
-    c_t.start()
+    for j in (3, 1, 2, 0):
+        c_t(j).start()
     do_term(0, (0,))
     have(1, do_y2)
     have(3, do_y1)
-    do_y2(0)
-    c_t.wait_recv()
     for j in (3, 1, 2, 0):
         turn = (x, x1, x3, x2)[j]
+        c_t(j).wait_recv()
         got = (term[0, :, turn] + termr[:, turn]).reshape(128, 256)
         if j == 0:
             wx0[...] = got
         else:
             wxs[j] = got.astype(BF16)
             c_wx(j).start()
+    do_y2(0)
     have(2, do_z)
-
     do_dq(1)
+    have(3, do_y2)
+    do_dq(2)
+    have(1, do_z)
+
+    pl.semaphore_wait(hop.at[3], 1)
+    got = wx0[...]
+    w_all(wxr.at[1:4], r_wx.at[0])
+    for j in (1, 2, 3):
+        got = got + wxr[j].astype(F32)
+    got = got.reshape(16, 8, 256)
+    for k in (0, 1):
+        rows = slice(4 * k, 4 * k + 4)
+        wz[16 * k : 16 * k + 16] = jnp.concatenate([got[:, rows, 0:128], got[:, rows, 128:256]], axis=1)
+    far_first = (8, 7, 9, 6, 10, 5, 11, 4, 12, 3, 13, 2, 14, 1, 15)
+    for d in far_first:
+        for k in (0, 1):
+            c_wz(k, d).start()
+    c_wz(1, 0).start()
+    have(3, do_z)
+
     c_dh(1).wait_recv()
     dqs[1, 64:128, :] += dqh[1]
     c_dq(1).start()
-    do_dq(2)
     c_dh(0).wait_recv()
     dqs[2, 0:64, :] += dqh[0]
     c_dq(2).start()
-    have(3, do_y2)
-    have(1, do_z)
     do_z(0)
     do_dq(0)
-
-    pl.semaphore_wait(hop.at[2], 2)
-    got = wx0[...]
-    for j in (1, 2, 3):
-        c_wx(j).wait_recv()
-        got = got + wxr[j].astype(F32)
-    wz[...] = got.reshape(16, 8, 256)
-
-    def go(d, carry):
-        c_wz(d).start()
-        return carry
-
-    lax.fori_loop(1, 16, go, 0)
-    have(3, do_z)
 
     def wait_z(d, carry):
         c_zr(d).wait_recv()
@@ -419,72 +426,54 @@
     for j in (1, 2, 3):
         c_f(j).start()
 
-    c_dq(1).wait_recv()
-    c_dq(2).wait_recv()
+    def drain(s):
+        if s < 3:
+
+            @pl.when(more > 0)
+            def _():
+                c_kz(s).wait_send()
+
+        c_kd(s).wait_send()
+        c_d(s).wait_send()
+        w_all(y1s.at[s], s_y1.at[s])
+        w_all(y2s.at[s], s_y2.at[s])
+        if s > 0:
+            c_z(s).wait_send()
+
+    for s in range(4):
+        have(s, drain)
+    w_all(qb.at[0:2], s_q.at[0])
+    w_all(qb.at[0], s_q.at[1])
+    w_all(st.at[1:3], s_st.at[0])
+    c_st(3).wait_send()
+    w_all(dqs.at[3], s_dh.at[0])
+    w_all(termr, s_t.at[0])
+    w_all(wxs.at[1:4], s_wx.at[0])
+
+    w_all(dqr, r_dq.at[0])
     o_main[...] = dqs[0, :, 0:512] + dqr[0, :, 0:512] + dqr[1, :, 0:512]
     o_rot[...] = dqs[0, :, 512:768] + dqr[0, :, 512:768] + dqr[1, :, 512:768]
 
-    def wait_wz(d, total):
-        c_wz(d).wait_recv()
-        return total + wzr[d]
-
-    wf[...] = lax.fori_loop(1, 16, wait_wz, wz[z])
-    c_wf.start()
+    w_all(fin.at[1:4], r_f.at[0])
     for j in range(4):
-        if j > 0:
-            c_f(j).wait_recv()
         rows = pl.ds(pl.multiple_of((y, y1, y3, y2)[j] * 32, 32), 32)
         got = zs[0] if j == 0 else fin[j].astype(F32)
         o_lat[rows, :] = got[:, 0:512]
         krots[rows, :] = got[:, 512:640]
     o_krot[...] = krots[...].T[0:64, :]
-    c_wf.wait_recv()
-
-    @pl.when(c == 0)
-    def _():
-        o_weight[:, 0:256] = wf[0:4, :]
-        o_weight[:, 256:512] = wfr[0:4, :]
-
-    @pl.when(c == 1)
-    def _():
-        o_weight[:, 0:256] = wfr[4:8, :]
-        o_weight[:, 256:512] = wf[4:8, :]
-
-    def drain(s):
-        if s < 3:
-
-            @pl.when(more > 0)
-            def _():
-                c_kz(s).wait_send()
-
-        c_kd(s).wait_send()
-        c_d(s).wait_send()
-        for g in (0, 1):
-            c_y1(s, g).wait_send()
-            c_y2(s, g).wait_send()
-        if s > 0:
-            c_z(s).wait_send()
-
-    for s in range(4):
-        have(s, drain)
-    c_t.wait_send()
-    c_wf.wait_send()
-    for i in (0, 1):
-        for p in (0, 1):
-            c_q(1 + i, p).wait_send()
-            c_qh(i, p).wait_send()
-        c_dh(i).wait_send()
-        c_dq(1 + i).wait_send()
-    for j in (1, 2, 3):
-        c_st(j).wait_send()
-        c_wx(j).wait_send()
-        c_f(j).wait_send()
-
-    def drain_wz(d, carry):
-        c_wz(d).wait_send()
-        return carry
-
-    lax.fori_loop(1, 16, drain_wz, 0)
+    w_all(dqs.at[1:3], s_dq.at[0])
+    w_all(fin.at[1:4], s_f.at[0])
+    w_all(wz.at[1:32], s_wz.at[0])
+
+    w_all(wzr.at[1:32], r_wz.at[0])
+    sums = [wz[16 * c + z] + wzr[1:16].sum(axis=0), wzr[16:32].sum(axis=0)]
+    for core in (0, 1):
+
+        @pl.when(c == core)
+        def _(core=core):
+            for k, at in ((0, core), (1, 1 - core)):
+                o_weight[:, 256 * at : 256 * at + 128] = sums[k][0:4, :]
+                o_weight[:, 256 * at + 128 : 256 * at + 256] = sums[k][4:8, :]
 
 
 def put_out(*refs):
@@ -502,8 +491,7 @@
     dma = pltpu.SemaphoreType.DMA
     scratch = [
         pltpu.VMEM((128, 128), F32),
-        pltpu.VMEM((512, 512), BF16),
-        pltpu.VMEM((512, 512), BF16),
+        pltpu.VMEM((2, 512, 512), BF16),
         pltpu.VMEM((128, 512), BF16),
         pltpu.VMEM((4, 128), F32),
         pltpu.VMEM((64, 128), BF16),
@@ -531,27 +519,24 @@
         pltpu.VMEM((128, 256), F32),
         pltpu.VMEM((4, 128, 256), BF16),
         pltpu.VMEM((4, 128, 256), BF16),
-        pltpu.VMEM((16, 8, 256), F32),
-        pltpu.VMEM((16, 8, 256), F32),
-        pltpu.VMEM((8, 256), F32),
-        pltpu.VMEM((8, 256), F32),
-        dma((12,)),
-        pltpu.SemaphoreType.REGULAR((3,)),
-        dma((5, 2)), dma((5, 2)),
-        dma((4,)), dma((4,)),
-        dma((4,)), dma((5,)),
+        pltpu.VMEM((32, 8, 128), F32),
+        pltpu.VMEM((32, 8, 128), F32),
+        dma((6,)),
+        pltpu.SemaphoreType.REGULAR((4,)),
+        dma((2,)), dma((3,)),
+        dma((2,)), dma((2,)),
+        dma((3,)), dma((3,)),
         dma((4,)), dma((4,)),
         dma((4,)), dma((4,)),
-        dma((4, 2)), dma((4, 2)),
-        dma((4, 2)), dma((4, 2)),
         dma((4,)), dma((4,)),
         dma((4,)), dma((4,)),
-        dma((2,)), dma((2,)),
         dma((3,)), dma((3,)),
-        dma, dma,
-        dma((4,)), dma((4,)),
-        dma((16,)), dma((16,)),
-        dma, dma,
+        dma((1,)), dma((1,)),
+        dma((1,)), dma((2,)),
+        dma((1,)), dma((1,)),
+        dma((1,)), dma((4,)),
+        dma((1,)), dma((1,)),
+        dma((1,)), dma((1,)),
     ]
     got = pl.pallas_call(
         body,

time: 61.4 us -> 58.1 us (0.946)
  Pallas kernels: 60.4 us -> 57.1 us
    pallas_call x1, Pallas kernels: 59.5 us -> 56.3 us  [per_device(): pl.pallas_call(body, out_shape=(pltpu.VMEM((128, 512), F32), pltpu.VMEM((...]
where the time goes in v5:
time: 58.1 us; the launch traced here: 57.9 us
  Pallas kernels  57.1 us (98%)
  between operations  0.8 us (1%)
    pallas_call x1, Pallas kernels, per_device(): pl.pallas_call(body, out_shape=(pltpu.VMEM((128, 512), F32), pltpu.VMEM((...  56.3 us

profile of v5, /device:TPU:1, one launch (start us, length us, event | category | flops | bytes accessed | tf_op | source)
XLA Modules:
  0.0 57.9 jit_solution(7272855367070651441)
XLA Ops:
  0.6 56.3 %shard_map.128 = (f32[128,512]{1,0:T(8,128)S(1)}, f32[128,256]{1,0:T(8,128)S(1)}, f32[128,512]{1,0:T(8,128)S(1)}, f32[64,128]{1,0:T(8,128)S(1)}, f32[4,512]{1,0:T(4,128)S(1)}) custom-call(bf16[128,512]{1,0:T(8,128)(2,1)} %qm.1, bf16[128,256]{1,0:T(8,128)(2,1)} %qr.1, bf16[128,512]{1,0:T(8,128)(2,1)} %lat.1, bf16[64,128]{1,0:T(8,128)(2,1)} %bitcast.2, ...), custom_call_target="tpu_custom_call" | custom-call | tf_op jit(solution)/shard_map/pallas_call | solution.py:541
  56.9 0.9 %shard_map.129 = (f32[128,512]{1,0:T(8,128)}, f32[128,256]{1,0:T(8,128)}, f32[128,512]{1,0:T(8,128)}, f32[64,128]{1,0:T(8,128)}, f32[4,512]{1,0:T(4,128)}) custom-call(f32[128,512]{1,0:T(8,128)S(1)} %get-tuple-element.15.refs_0_, f32[128,256]{1,0:T(8,128)S(1)} %get-tuple-element.16.refs_1_, f32[128,512]{1,0:T(8,128)S(1)} %get-tuple-element.17.refs_2_, ...), custom_call_target="tpu_custom_call" | custom-call | tf_op jit(solution)/shard_map/pallas_call | solution.py:557

commit v6 on v5

--- a/solution.py
+++ b/solution.py
@@ -31,7 +31,7 @@
 def body(
     qm, qr, lat, krt, kwh, vwh, hoh, og, lsh,
     o_main, o_rot, o_lat, o_krot, o_weight,
-    krots, kv, ho, ls, krv, qb, st, sts, qc, gr, keys, mix, part, dsum, y1s, y1r, y2s, y2r, zs, zr, fin,
+    krots, kv, ho, ls, krv, qb, st, sts, qc, qt, gr, keys, mix, part, turned, dsum, y1s, y1r, y2s, y2r, zs, zr, fin,
     dqs, dqh, dqr, term, termr, wx0, wxs, wxr, wz, wzr,
     s_loc, hop, s_q, r_q, s_st, r_st, s_kz, r_kz, s_kd, r_kd, s_d, r_d, s_y1, r_y1, s_y2, r_y2,
     s_z, r_z, s_f, r_f, s_dh, r_dh, s_dq, r_dq, s_t, r_t, s_wx, r_wx, s_wz, r_wz,
@@ -100,7 +100,7 @@
 
     def c_t(j):
         turn = (x, x1, x3, x2)[j]
-        return remote(term.at[1, :, turn], termr.at[:, turn], s_t.at[0], r_t.at[j], sib)
+        return remote(term.at[1 - c, :, turn], termr.at[:, turn], s_t.at[0], r_t.at[j], sib)
 
     def c_wx(j):
         return remote(wxs.at[j], wxr.at[j], s_wx.at[0], r_wx.at[0], xdev[j])
@@ -195,12 +195,14 @@
             qc[slot, rows, 0:512] = dot(qb[j, p, :, k * 128 : k * 128 + 128], kw[:, cols], NT).astype(BF16)
             gr[slot, rows, :] = dot(qb[j, p, :, 384 + k * 128 : 512 + k * 128], vw[:, cols], NT).astype(BF16)
             rot = qb[j, p, :, 256 + k * 64 : 320 + k * 64]
+            qt[slot, :, rows] = rot.T
             qc[slot, rows, 512:WIDE] = jnp.concatenate([rot, jnp.zeros((128, 64), BF16)], axis=1)
             sts[slot, 0:2, rows] = st[j, 0:2, cols]
 
     project(0)
     mix[...] = jnp.zeros_like(mix)
     part[...] = jnp.zeros_like(part)
+    turned[...] = jnp.zeros_like(turned)
 
     def tile(s, j, masked):
         kt = keys[s].reshape(256, WIDE)
@@ -223,9 +225,8 @@
         d_low = dscores.astype(BF16)
         mix[j, 0:576, :] += dot(kt[:, 0:576], d_low, TN)
         main = factor * dot(d_low, qc[j, :, 0:512]) + dot(w_low, gr[j])
-        rest = factor * dot(d_low, qc[j, :, 512:WIDE])
         part[s, :, :, 0:512] += main.reshape(2, 128, 512)
-        part[s, :, :, 512:WIDE] += rest.reshape(2, 128, 128)
+        turned[s] += factor * dot(qt[j], d_low, NT)
 
     def own(s, g, yy):
         rows = pl.ds(pl.multiple_of(yy * 32 + 16 * g, 16), 16)
@@ -297,15 +298,19 @@
             c_qh(i, p).start()
 
     def give(s):
-        c_d(s).start()
+        for k in (1, 0):
+            rot = turned[s, :, 128 * k : 128 * k + 128].T
+            part[s, k, :, 512:WIDE] = jnp.concatenate([rot, jnp.zeros((128, 64), F32)], axis=1)
+            if k == 1:
+                c_d(s).start()
 
     ready(0)
     run((0, 0))
+    c_q(1, 1).start()
+    c_q(2, 1).start()
     pl.semaphore_wait(hop.at[0], 6)
     relay(1)
     have(1, arrive)
-    c_q(1, 1).start()
-    c_q(2, 1).start()
     have(1, ready)
     run((1, 0))
     halves(0)
@@ -321,20 +326,18 @@
     have(2, arrive)
     run((1, 2))
     have(2, ready)
-    run((2, 0), (2, 1), (2, 2))
+    run((2, 0), (2, 1))
     pl.semaphore_wait(hop.at[2], 2)
     pl.semaphore_signal(hop.at[3], inc=1, device_id=sib, device_id_type=MESH)
     w_all(qb.at[3], r_q.at[2])
     c_st(3).wait_recv()
     project(3)
+    run((2, 3))
     have(3, arrive)
-    run((2, 3))
-    have(2, give)
     run((1, 3))
     have(1, give)
     run((0, 3))
     give(0)
-    have(2, do_y1)
     have(3, ready)
     run((3, 3))
     do_dq(3)
@@ -343,52 +346,55 @@
     have(1, do_y1)
     run((3, 1))
     do_y1(0)
-    run((3, 2))
-    have(2, do_y2)
-
-    def do_term(rel, slots):
-        p = c if rel == 0 else 1 - c
+
+    def do_term(p, slots, fresh):
         for k in (0, 1):
             got = jnp.zeros((512, 128), F32)
-            wide = pl.ds(pl.multiple_of((2 * p + k) * 128, 128), 128)
             for j in slots:
-                if j in (0, 3):
-                    m = mix[j, 0:512, wide]
-                else:
-                    m = mix[1 + p, 0:512, (2 * (j - 1) + k) * 128 : (2 * (j - 1) + k + 1) * 128]
+                slot, b = place_of(j, 2 * p + k)
+                m = mix[slot, 0:512, b * 128 : b * 128 + 128]
                 high = m.astype(BF16)
                 rest = (m - high.astype(F32)).astype(BF16)
                 q = qb[j, p, :, k * 128 : k * 128 + 128]
                 got = got + dot(jnp.concatenate([high, rest], axis=1), jnp.concatenate([q, q], axis=0))
             got = (factor * got).reshape(16, 4, 8, 128)
-            if slots == (0,):
-                got = got + term[rel, :, :, :, k * 128 : (k + 1) * 128]
-            term[rel, :, :, :, k * 128 : (k + 1) * 128] = got
-
-    do_term(1, (1, 2, 3))
-    do_term(0, (1, 2, 3))
+            if not fresh:
+                got = got + term[p, :, :, :, k * 128 : (k + 1) * 128]
+            term[p, :, :, :, k * 128 : (k + 1) * 128] = got
+
+    def hand_over(core):
+        @pl.when(c == core)
+        def _():
+            for j in (3, 1, 2, 0):
+                c_t(j).start()
+
+    do_term(0, (1, 2, 3), True)
     run((3, 0))
+    do_term(0, (0,), False)
+    hand_over(1)
+    do_term(1, (0, 3), True)
+    run((3, 2))
     have(3, give)
-    do_term(1, (0,))
-    for j in (3, 1, 2, 0):
-        c_t(j).start()
-    do_term(0, (0,))
+    run((2, 2))
+    do_term(1, (1, 2), False)
+    hand_over(0)
+    have(3, do_y1)
+    have(2, give)
     have(1, do_y2)
-    have(3, do_y1)
     for j in (3, 1, 2, 0):
         turn = (x, x1, x3, x2)[j]
         c_t(j).wait_recv()
-        got = (term[0, :, turn] + termr[:, turn]).reshape(128, 256)
+        got = (term[c, :, turn] + termr[:, turn]).reshape(128, 256)
         if j == 0:
             wx0[...] = got
         else:
             wxs[j] = got.astype(BF16)
             c_wx(j).start()
+    have(2, do_y1)
     do_y2(0)
-    have(2, do_z)
     do_dq(1)
+    do_dq(2)
     have(3, do_y2)
-    do_dq(2)
     have(1, do_z)
 
     pl.semaphore_wait(hop.at[3], 1)
@@ -406,6 +412,7 @@
             c_wz(k, d).start()
     c_wz(1, 0).start()
     have(3, do_z)
+    have(2, do_y2)
 
     c_dh(1).wait_recv()
     dqs[1, 64:128, :] += dqh[1]
@@ -415,6 +422,7 @@
     c_dq(2).start()
     do_z(0)
     do_dq(0)
+    have(2, do_z)
 
     def wait_z(d, carry):
         c_zr(d).wait_recv()
@@ -499,10 +507,12 @@
         pltpu.VMEM((4, 8, 512), F32),
         pltpu.VMEM((4, 8, 512), F32),
         pltpu.VMEM((4, 512, WIDE), BF16),
+        pltpu.VMEM((4, 64, 512), BF16),
         pltpu.VMEM((4, 512, 512), BF16),
         pltpu.VMEM((4, 2, 128, WIDE), BF16),
         pltpu.VMEM((4, WIDE, 512), F32),
         pltpu.VMEM((4, 2, 128, WIDE), F32),
+        pltpu.VMEM((4, 64, 256), F32),
         pltpu.VMEM((4, 128, WIDE), F32),
         pltpu.VMEM((4, 2, 2, 16, WIDE), BF16),
         pltpu.VMEM((4, 2, 2, 16, WIDE), BF16),

time: 58.1 us -> 57.7 us (level)
  no operation moved by 1% of the time
where the time goes in v6:
time: 57.7 us; the launch traced here: 57.5 us
  Pallas kernels  56.7 us (98%)
  between operations  0.8 us (1%)
    pallas_call x1, Pallas kernels, per_device(): pl.pallas_call(body, out_shape=(pltpu.VMEM((128, 512), F32), pltpu.VMEM((...  55.8 us

profile of v6, /device:TPU:1, one launch (start us, length us, event | category | flops | bytes accessed | tf_op | source)
XLA Modules:
  0.0 57.5 jit_solution(4521143612527994900)
XLA Ops:
  0.6 55.8 %shard_map.128 = (f32[128,512]{1,0:T(8,128)S(1)}, f32[128,256]{1,0:T(8,128)S(1)}, f32[128,512]{1,0:T(8,128)S(1)}, f32[64,128]{1,0:T(8,128)S(1)}, f32[4,512]{1,0:T(4,128)S(1)}) custom-call(bf16[128,512]{1,0:T(8,128)(2,1)} %qm.1, bf16[128,256]{1,0:T(8,128)(2,1)} %qr.1, bf16[128,512]{1,0:T(8,128)(2,1)} %lat.1, bf16[64,128]{1,0:T(8,128)(2,1)} %bitcast.2, ...), custom_call_target="tpu_custom_call" | custom-call | tf_op jit(solution)/shard_map/pallas_call | solution.py:551
  56.5 0.9 %shard_map.129 = (f32[128,512]{1,0:T(8,128)}, f32[128,256]{1,0:T(8,128)}, f32[128,512]{1,0:T(8,128)}, f32[64,128]{1,0:T(8,128)}, f32[4,512]{1,0:T(4,128)}) custom-call(f32[128,512]{1,0:T(8,128)S(1)} %get-tuple-element.15.refs_0_, f32[128,256]{1,0:T(8,128)S(1)} %get-tuple-element.16.refs_1_, f32[128,512]{1,0:T(8,128)S(1)} %get-tuple-element.17.refs_2_, ...), custom_call_target="tpu_custom_call" | custom-call | tf_op jit(solution)/shard_map/pallas_call | solution.py:567

commit v7 on v6

--- a/solution.py
+++ b/solution.py
@@ -378,18 +378,25 @@
     run((2, 2))
     do_term(1, (1, 2), False)
     hand_over(0)
+
+    def over_x(core):
+        @pl.when(c == core)
+        def _():
+            for j in (3, 1, 2, 0):
+                turn = (x, x1, x3, x2)[j]
+                c_t(j).wait_recv()
+                got = (term[core, :, turn] + termr[:, turn]).reshape(128, 256)
+                if j == 0:
+                    wx0[...] = got
+                else:
+                    wxs[j] = got.astype(BF16)
+                    c_wx(j).start()
+
+    over_x(0)
     have(3, do_y1)
     have(2, give)
     have(1, do_y2)
-    for j in (3, 1, 2, 0):
-        turn = (x, x1, x3, x2)[j]
-        c_t(j).wait_recv()
-        got = (term[c, :, turn] + termr[:, turn]).reshape(128, 256)
-        if j == 0:
-            wx0[...] = got
-        else:
-            wxs[j] = got.astype(BF16)
-            c_wx(j).start()
+    over_x(1)
     have(2, do_y1)
     do_y2(0)
     do_dq(1)

time: 57.7 us -> 57 us (0.988)
  Pallas kernels: 56.7 us -> 56 us
    pallas_call x1, Pallas kernels: 55.8 us -> 55.2 us  [per_device(): pl.pallas_call(body, out_shape=(pltpu.VMEM((128, 512), F32), pltpu.VMEM((...]
where the time goes in v7:
time: 57 us; the launch traced here: 56.8 us
  Pallas kernels  56 us (98%)
  between operations  0.8 us (1%)
    pallas_call x1, Pallas kernels, per_device(): pl.pallas_call(body, out_shape=(pltpu.VMEM((128, 512), F32), pltpu.VMEM((...  55.2 us

profile of v7, /device:TPU:1, one launch (start us, length us, event | category | flops | bytes accessed | tf_op | source)
XLA Modules:
  0.0 56.8 jit_solution(11271074327347360175)
XLA Ops:
  0.6 55.2 %shard_map.128 = (f32[128,512]{1,0:T(8,128)S(1)}, f32[128,256]{1,0:T(8,128)S(1)}, f32[128,512]{1,0:T(8,128)S(1)}, f32[64,128]{1,0:T(8,128)S(1)}, f32[4,512]{1,0:T(4,128)S(1)}) custom-call(bf16[128,512]{1,0:T(8,128)(2,1)} %qm.1, bf16[128,256]{1,0:T(8,128)(2,1)} %qr.1, bf16[128,512]{1,0:T(8,128)(2,1)} %lat.1, bf16[64,128]{1,0:T(8,128)(2,1)} %bitcast.2, ...), custom_call_target="tpu_custom_call" | custom-call | tf_op jit(solution)/shard_map/pallas_call | solution.py:558
  55.8 0.9 %shard_map.129 = (f32[128,512]{1,0:T(8,128)}, f32[128,256]{1,0:T(8,128)}, f32[128,512]{1,0:T(8,128)}, f32[64,128]{1,0:T(8,128)}, f32[4,512]{1,0:T(4,128)}) custom-call(f32[128,512]{1,0:T(8,128)S(1)} %get-tuple-element.15.refs_0_, f32[128,256]{1,0:T(8,128)S(1)} %get-tuple-element.16.refs_1_, f32[128,512]{1,0:T(8,128)S(1)} %get-tuple-element.17.refs_2_, ...), custom_call_target="tpu_custom_call" | custom-call | tf_op jit(solution)/shard_map/pallas_call | solution.py:574

commit v8 on v7

--- a/solution.py
+++ b/solution.py
@@ -345,7 +345,6 @@
     c_dh(1).start()
     have(1, do_y1)
     run((3, 1))
-    do_y1(0)
 
     def do_term(p, slots, fresh):
         for k in (0, 1):
@@ -398,7 +397,7 @@
     have(1, do_y2)
     over_x(1)
     have(2, do_y1)
-    do_y2(0)
+    do_y1(0)
     do_dq(1)
     do_dq(2)
     have(3, do_y2)
@@ -420,6 +419,7 @@
     c_wz(1, 0).start()
     have(3, do_z)
     have(2, do_y2)
+    do_y2(0)
 
     c_dh(1).wait_recv()
     dqs[1, 64:128, :] += dqh[1]
@@ -427,9 +427,9 @@
     c_dh(0).wait_recv()
     dqs[2, 0:64, :] += dqh[0]
     c_dq(2).start()
-    do_z(0)
     do_dq(0)
     have(2, do_z)
+    do_z(0)
 
     def wait_z(d, carry):
         c_zr(d).wait_recv()

time: 57 us -> 57.8 us (1.014); the launches traced: 56.8 us -> 56.8 us
  no operation moved by 1% of the time
where the time goes in v8:
time: 57.8 us; the launch traced here: 56.8 us
  Pallas kernels  56 us (97%)
  between operations  0.8 us (1%)
    pallas_call x1, Pallas kernels, per_device(): pl.pallas_call(body, out_shape=(pltpu.VMEM((128, 512), F32), pltpu.VMEM((...  55.1 us

profile of v8, /device:TPU:1, one launch (start us, length us, event | category | flops | bytes accessed | tf_op | source)
XLA Modules:
  0.0 56.8 jit_solution(11639789374323684618)
XLA Ops:
  0.6 55.1 %shard_map.128 = (f32[128,512]{1,0:T(8,128)S(1)}, f32[128,256]{1,0:T(8,128)S(1)}, f32[128,512]{1,0:T(8,128)S(1)}, f32[64,128]{1,0:T(8,128)S(1)}, f32[4,512]{1,0:T(4,128)S(1)}) custom-call(bf16[128,512]{1,0:T(8,128)(2,1)} %qm.1, bf16[128,256]{1,0:T(8,128)(2,1)} %qr.1, bf16[128,512]{1,0:T(8,128)(2,1)} %lat.1, bf16[64,128]{1,0:T(8,128)(2,1)} %bitcast.2, ...), custom_call_target="tpu_custom_call" | custom-call | tf_op jit(solution)/shard_map/pallas_call | solution.py:558
  55.7 0.9 %shard_map.129 = (f32[128,512]{1,0:T(8,128)}, f32[128,256]{1,0:T(8,128)}, f32[128,512]{1,0:T(8,128)}, f32[64,128]{1,0:T(8,128)}, f32[4,512]{1,0:T(4,128)}) custom-call(f32[128,512]{1,0:T(8,128)S(1)} %get-tuple-element.15.refs_0_, f32[128,256]{1,0:T(8,128)S(1)} %get-tuple-element.16.refs_1_, f32[128,512]{1,0:T(8,128)S(1)} %get-tuple-element.17.refs_2_, ...), custom_call_target="tpu_custom_call" | custom-call | tf_op jit(solution)/shard_map/pallas_call | solution.py:574
